TPU v7x, 32 devices: a whole 2x2x4 slice. The times are simulated.
32 devices in a mesh: ep: 8 (over z, core), tp: 4 (over y, x).
Axes of the slice: x: 2, y: 2, z: 4, core: 2. Of those that a mesh axis runs over, the one named last changes fastest.
Arguments:
- mix_input: bfloat16 [1024, 2048], P('ep'), may hold values from -8 to 8
- expert_input: bfloat16 [1024, 2048], P('ep'), may hold values from -8 to 8
- mix_gain: float32 [2048], replicated, may hold values from 0.1 to 1.9
- moe_gain: float32 [2048], replicated, may hold values from 0.1 to 1.9
- pool_in: bfloat16 [2048, 1024], P(None, 'tp'), may hold values from -0.125 to 0.125
- pool_scale: float32 [1024], P('tp'), may hold values from 0.25 to 10
- pool_gain: float32 [1024], P('tp'), may hold values from 0.1 to 1.9
- pool_out: bfloat16 [1024, 2048], P(None, 'tp'), may hold values from -0.1875 to 0.1875
- route: int32 [1024, 4], P('ep'), may hold values from 0 to 7, all different within a row; in each aligned block of 128 rows (0 to 127, 128 to 255, ...) at most 128 rows name the same one
- route_score: float32 [1024, 4], P('ep'), may hold values from 0.05 to 1
- expert_gate: bfloat16 [8, 2048, 2048], P('ep', None, 'tp'), may hold values from -0.125 to 0.125
- expert_up: bfloat16 [8, 2048, 2048], P('ep', None, 'tp'), may hold values from -0.125 to 0.125
- expert_down: bfloat16 [8, 2048, 2048], P('ep', 'tp'), may hold values from -0.1875 to 0.1875
- shared_gate: bfloat16 [2048, 2048], P(None, 'tp'), may hold values from -0.125 to 0.125
- shared_up: bfloat16 [2048, 2048], P(None, 'tp'), may hold values from -0.125 to 0.125
- shared_down: bfloat16 [2048, 2048], P(None, 'tp'), may hold values from -0.125 to 0.125
Outputs:
- mix_out: bfloat16 [1024, 2048], P('ep', 'tp')
- moe_out: bfloat16 [1024, 2048], P('ep', 'tp')
Inputs may be any that keep to these rules, and one draw needn't show every extreme that they name: `route`: each row names 4 different experts. In the rows of one index of ep (aligned blocks of 128 rows) no expert is named more than 128 times, a bound that some block reaches.
All inputs are finite; a program needn't handle non-finite values.
Results may differ from a plain program's by a relative error of at most 0.014.
Values may be sent and summed in bfloat16 or wider, within the bound.
A program may use at most 64 MiB of HBM per device.

v0:
```python
import jax
import jax.numpy as jnp
from jax import lax
from jax.experimental import pallas as pl
from jax.experimental.pallas import tpu as pltpu
from jax.sharding import PartitionSpec as P

epsilon = 1e-06
reach_rows = 15
window_widths = (2, 4, 8, 16)


def shifted(block, axis, distance):
    devices = range(lax.axis_size(axis))
    route = [(i - distance, i) for i in devices if i - distance in devices]
    return lax.ppermute(block, axis, route)


def row_norm(rows, gain):
    values = rows.astype(jnp.float32)
    scale = lax.rsqrt(jnp.mean(values * values, axis=-1, keepdims=True) + epsilon)
    return (values * scale * gain).astype(jnp.bfloat16)


def window_means(extended, position, group, n_rows):
    total = jnp.zeros((n_rows, extended.shape[1]), jnp.float32)
    result = jnp.zeros((n_rows, extended.shape[1]), jnp.float32)
    for lag in range(16):
        total = total + extended[reach_rows - lag : reach_rows - lag + n_rows]
        for index, width in enumerate(window_widths):
            if lag + 1 == width:
                count = jnp.minimum(position, float(width))[:, None]
                result = jnp.where(group[None, :] == index, total / count, result)
    return result - extended[reach_rows:]


def serve(sending, expert_gate, expert_up, expert_down):
    arrived = lax.all_to_all(sending, "ep", split_axis=0, concat_axis=0, tiled=True)
    gate = jnp.einsum("send,edf->senf", arrived, expert_gate, preferred_element_type=jnp.float32)
    upper = jnp.einsum("send,edf->senf", arrived, expert_up, preferred_element_type=jnp.float32)
    hidden = (jax.nn.silu(gate) * upper).astype(jnp.bfloat16)
    term = jnp.einsum("senf,efd->send", hidden, expert_down, preferred_element_type=jnp.float32)
    summed = lax.psum_scatter(term.astype(jnp.bfloat16), "tp", scatter_dimension=3, tiled=True)
    return lax.all_to_all(summed, "ep", split_axis=0, concat_axis=0, tiled=True)


def on_device(
    mix_input,
    expert_input,
    mix_gain,
    moe_gain,
    pool_in,
    pool_scale,
    pool_gain,
    pool_out,
    route,
    route_score,
    expert_gate,
    expert_up,
    expert_down,
    shared_gate,
    shared_up,
    shared_down,
):
    tok_rows = mix_input.shape[0]
    channels = pool_in.shape[1]
    pool_width = channels * lax.axis_size("tp")
    mix_norm = row_norm(mix_input, mix_gain)
    pool_input = jnp.dot(mix_norm, pool_in, preferred_element_type=jnp.float32).astype(jnp.bfloat16)
    before = shifted(pool_input[tok_rows - reach_rows :], "ep", 1)
    extended = jnp.concatenate([before, pool_input], axis=0).astype(jnp.float32)
    position = (lax.axis_index("ep") * tok_rows + jnp.arange(tok_rows, dtype=jnp.int32) + 1).astype(
        jnp.float32
    )
    channel_ids = lax.axis_index("tp") * channels + jnp.arange(channels, dtype=jnp.int32)
    group = channel_ids // (pool_width // 4)
    scaled = window_means(extended, position, group, tok_rows) * pool_scale
    squares = lax.psum(jnp.sum(scaled * scaled, axis=1), "tp")
    pooled_norm = (scaled * lax.rsqrt(squares / pool_width + epsilon)[:, None] * pool_gain).astype(
        jnp.bfloat16
    )
    moe_norm = row_norm(expert_input, moe_gain)
    shared_hidden = (
        jax.nn.silu(jnp.dot(moe_norm, shared_gate, preferred_element_type=jnp.float32))
        * jnp.dot(moe_norm, shared_up, preferred_element_type=jnp.float32)
    ).astype(jnp.bfloat16)
    pooled_all, shared_all = (
        lax.all_gather(pooled_norm, "tp", axis=1, tiled=True),
        lax.all_gather(shared_hidden, "tp", axis=1, tiled=True),
    )
    mix_out = jnp.dot(pooled_all, pool_out, preferred_element_type=jnp.float32).astype(jnp.bfloat16)
    shared_part = jnp.dot(shared_all, shared_down, preferred_element_type=jnp.float32)
    n_tok, top = route.shape
    local_experts = expert_gate.shape[0]
    experts = local_experts * lax.axis_size("ep")
    capacity = 2 * n_tok * top // experts
    flat_route = route.reshape(-1)
    table = (flat_route[:, None] == jnp.arange(experts, dtype=jnp.int32)[None, :]).astype(jnp.int32)
    ranks = jnp.sum((jnp.cumsum(table, axis=0) - table) * table, axis=1)
    slot = flat_route * capacity + ranks
    owner = (
        jnp.full((experts * capacity,), n_tok, jnp.int32)
        .at[slot]
        .set(jnp.arange(n_tok * top, dtype=jnp.int32) // top)
    )
    padded_rows = jnp.concatenate(
        [moe_norm, jnp.zeros((1, moe_norm.shape[1]), jnp.bfloat16)], axis=0
    )
    outgoing = padded_rows[owner].reshape(
        lax.axis_size("ep"), local_experts, capacity, moe_norm.shape[1]
    )
    middle = capacity // 2
    first = serve(outgoing[:, :, :middle], expert_gate, expert_up, expert_down)
    second = serve(outgoing[:, :, middle:], expert_gate, expert_up, expert_down)
    returned = jnp.concatenate([first, second], axis=2)
    back_rows = returned.reshape(experts * capacity, returned.shape[3])
    picked = back_rows[slot].reshape(n_tok, top, returned.shape[3]).astype(jnp.float32)
    weights = 2.5 * route_score / jnp.sum(route_score, axis=1, keepdims=True)
    routed = jnp.sum(picked * weights[:, :, None], axis=1)
    moe_out = (routed + shared_part).astype(jnp.bfloat16)
    return (mix_out, moe_out)


MESH = pl.DeviceIdType.MESH


def places():
    ep, tp = lax.axis_index("ep"), lax.axis_index("tp")
    z, core = ep // 2, ep % 2
    y, x = tp // 2, tp % 2
    return ep, tp, z, core, y * 2 + 1 - x, (1 - y) * 2 + x, (1 - y) * 2 + 1 - x


def greet(partners):
    barrier = pltpu.get_barrier_semaphore()
    for partner in partners:
        pl.semaphore_signal(barrier, inc=1, device_id=partner, device_id_type=MESH)
    pl.semaphore_wait(barrier, len(partners))


def aligned(start, size):
    return pl.ds(pl.multiple_of(start * size, size), size)


def gather_kernel(n_ep, m_ref, w_ref, sg_ref, su_ref, g_ref, wg_ref, sh_ref, *sems):
    (w_s, w_r, z_s, z_r, x_s, x_r, y_s, y_r, dx_s, dx_r, dy_s, dy_r, c_s, c_r) = sems
    ep, tp, z, core, xn, yn, _ = places()
    n_z = n_ep // 2
    rows = m_ref.shape[0]
    cols = m_ref.shape[1] // 4
    half = rows // 2
    greet([((ep + m) % n_ep, tp) for m in range(1, n_ep)] + [(ep, xn), (ep, yn)])

    def send(src, dst, s, r, device):
        copy = pltpu.make_async_remote_copy(
            src_ref=src, dst_ref=dst, send_sem=s, recv_sem=r, device_id=device, device_id_type=MESH
        )
        copy.start()
        return copy

    own_rows = aligned(ep, rows)
    other_core = z * 2 + 1 - core
    order = [k for k in (1, n_z - 1)] + list(range(2, n_z - 1))
    z_copies = {}
    for k in order:
        target = ((z + k) % n_z) * 2 + core
        z_copies[k] = send(
            m_ref.at[:, aligned(tp, cols)],
            g_ref.at[own_rows, aligned(tp, cols)],
            z_s.at[k],
            z_r.at[k],
            (target, tp),
        )
    c_copies = {0: send(m_ref, g_ref.at[own_rows, :], c_s.at[0], c_r.at[0], (other_core, tp))}
    w_copies = [
        send(w_ref, wg_ref.at[ep], w_s.at[m], w_r.at[m], ((ep + m) % n_ep, tp))
        for m in range(1, n_ep)
    ]
    g_ref[own_rows, :] = m_ref[...]
    wg_ref[ep] = w_ref[...]
    tile = sg_ref.shape[1] // 2

    def shared_tile(index, carry):
        part = aligned(index, tile)
        gate = jnp.dot(m_ref[...], sg_ref[:, part], preferred_element_type=jnp.float32)
        upper = jnp.dot(m_ref[...], su_ref[:, part], preferred_element_type=jnp.float32)
        sh_ref[:, part] = (gate / (1.0 + jnp.exp(-gate)) * upper).astype(jnp.bfloat16)
        return carry

    lax.fori_loop(0, 2, shared_tile, 0)
    x_copies, y_copies, dx_copies, dy_copies = {}, {}, {}, {}

    def block(k):
        return ((z + n_z - k) % n_z) * 2 + core

    def piece(k, quarter):
        return g_ref.at[aligned(block(k), rows), aligned(quarter, cols)]

    def half_piece(k, part, quarter):
        start = pl.multiple_of(block(k) * rows + part * half, half)
        return g_ref.at[pl.ds(start, half), aligned(quarter, cols)]

    def across(k):
        z_copies[k].wait_recv()
        x_copies[k] = send(piece(k, tp), piece(k, tp), x_s.at[k], x_r.at[k], (ep, xn))
        y_copies[k] = send(piece(k, tp), piece(k, tp), y_s.at[k], y_r.at[k], (ep, yn))

    def corner(k):
        x_copies[k].wait_recv()
        dx_copies[k] = send(
            half_piece(k, 0, xn), half_piece(k, 0, xn), dx_s.at[k], dx_r.at[k], (ep, yn)
        )
        y_copies[k].wait_recv()
        dy_copies[k] = send(
            half_piece(k, 1, yn), half_piece(k, 1, yn), dy_s.at[k], dy_r.at[k], (ep, xn)
        )

    def over(k):
        dx_copies[k].wait_recv()
        dy_copies[k].wait_recv()
        whole = g_ref.at[aligned(block(k), rows), :]
        c_copies[k] = send(whole, whole, c_s.at[k], c_r.at[k], (other_core, tp))

    for index in range(len(order) + 2):
        if index < len(order):
            across(order[index])
        if 1 <= index < len(order) + 1:
            corner(order[index - 1])
        if index >= 2:
            over(order[index - 2])
    for k in [0] + order:
        c_copies[k].wait_recv()
    for copy in w_copies:
        copy.wait()
    for group in (z_copies, x_copies, y_copies, dx_copies, dy_copies, c_copies):
        for copy in group.values():
            copy.wait_send()


def gather_rows(moe_norm, dense, shared_gate, shared_up, n_ep):
    n_z = n_ep // 2
    sems = [pltpu.SemaphoreType.DMA((n_ep,))] * 2 + [pltpu.SemaphoreType.DMA((n_z,))] * 12
    vmem = pl.BlockSpec(memory_space=pltpu.VMEM)
    return pl.pallas_call(
        lambda *refs: gather_kernel(n_ep, *refs),
        out_shape=(
            jax.ShapeDtypeStruct((n_ep * moe_norm.shape[0], moe_norm.shape[1]), jnp.bfloat16),
            jax.ShapeDtypeStruct((n_ep,) + dense.shape, jnp.float32),
            jax.ShapeDtypeStruct((moe_norm.shape[0], shared_gate.shape[1]), jnp.bfloat16),
        ),
        in_specs=[vmem] * 4,
        out_specs=(vmem,) * 3,
        scratch_shapes=sems,
        compiler_params=pltpu.CompilerParams(collective_id=0, has_side_effects=True, vmem_limit_bytes=20 << 20),
    )(moe_norm, dense, shared_gate, shared_up)


def reduce_kernel(n_ep, h_ref, down_ref, sh_ref, po_ref, sq_ref, o_ref, sh_all, po_all, sq_all, *scratch):
    (p, ca, s, bx, by, qx, qy, r, bz) = scratch[:9]
    (c_s, c_r, dx_s, dx_r, dy_s, dy_r, x_s, x_r, y_s, y_r, z_s, z_r, t_s, t_r) = scratch[9:]
    ep, tp, z, core, xn, yn, dg = places()
    n_z = n_ep // 2
    rows = o_ref.shape[0]
    cols = o_ref.shape[1]
    half = rows // 2
    other_core = z * 2 + 1 - core
    peers = (xn, yn, dg)
    greet(
        [(other_core, tp)]
        + [(((z + k) % n_z) * 2 + core, tp) for k in range(1, n_z)]
        + [(ep, t) for t in peers]
    )

    def send(src, dst, sem_s, sem_r, device):
        copy = pltpu.make_async_remote_copy(
            src_ref=src, dst_ref=dst, send_sem=sem_s, recv_sem=sem_r, device_id=device, device_id_type=MESH
        )
        copy.start()
        return copy

    order = list(range(2, n_z - 1)) + [1, n_z - 1, 0]
    c_copies, dx_copies, dy_copies, x_copies, y_copies, z_copies = {}, {}, {}, {}, {}, {}

    def down(k):
        pair = aligned((z + k) % n_z, 2 * rows)

        def tile(index, carry):
            part = aligned(index, cols)
            p[k, :, part] = jnp.dot(
                h_ref[pair, :], down_ref[:, part], preferred_element_type=jnp.float32
            ).astype(jnp.bfloat16)
            return carry

        lax.fori_loop(0, down_ref.shape[1] // cols, tile, 0)
        c_copies[k] = send(
            p.at[k, aligned(1 - core, rows), :], ca.at[k], c_s.at[k], c_r.at[k], (other_core, tp)
        )

    low, high = pl.ds(0, half), pl.ds(half, half)

    def first(k):
        c_copies[k].wait_recv()
        s[k] = (
            p[k, aligned(core, rows), :].astype(jnp.float32) + ca[k].astype(jnp.float32)
        ).astype(jnp.bfloat16)
        dx_copies[k] = send(
            s.at[k, low, aligned(dg, cols)], bx.at[k], dx_s.at[k], dx_r.at[k], (ep, xn)
        )
        dy_copies[k] = send(
            s.at[k, high, aligned(dg, cols)], by.at[k], dy_s.at[k], dy_r.at[k], (ep, yn)
        )

    def second(k):
        dx_copies[k].wait_recv()
        s[k, low, aligned(yn, cols)] = (
            s[k, low, aligned(yn, cols)].astype(jnp.float32) + bx[k].astype(jnp.float32)
        ).astype(jnp.bfloat16)
        y_copies[k] = send(
            s.at[k, :, aligned(yn, cols)], qy.at[k], y_s.at[k], y_r.at[k], (ep, yn)
        )
        dy_copies[k].wait_recv()
        s[k, high, aligned(xn, cols)] = (
            s[k, high, aligned(xn, cols)].astype(jnp.float32) + by[k].astype(jnp.float32)
        ).astype(jnp.bfloat16)
        x_copies[k] = send(
            s.at[k, :, aligned(xn, cols)], qx.at[k], x_s.at[k], x_r.at[k], (ep, xn)
        )

    def third(k):
        x_copies[k].wait_recv()
        y_copies[k].wait_recv()
        total = (
            s[k, :, aligned(tp, cols)].astype(jnp.float32)
            + qx[k].astype(jnp.float32)
            + qy[k].astype(jnp.float32)
        )
        if k == 0:
            o_ref[...] = total
        else:
            r[k] = total.astype(jnp.bfloat16)
            target = ((z + k) % n_z) * 2 + core
            z_copies[k] = send(r.at[k], bz.at[k], z_s.at[k], z_r.at[k], (target, tp))

    t_copies = []
    down(order[0])
    for index in range(n_z + 2):
        if index + 1 < n_z:
            down(order[index + 1])
        if index < n_z:
            first(order[index])
        if 1 <= index < n_z + 1:
            second(order[index - 1])
        if index == n_z:
            for number, t in enumerate(peers):
                pairs = (
                    (sh_ref, sh_all.at[:, aligned(tp, sh_ref.shape[1])]),
                    (po_ref, po_all.at[:, aligned(tp, po_ref.shape[1])]),
                    (sq_ref, sq_all.at[tp]),
                )
                for kind, (src, dst) in enumerate(pairs):
                    t_copies.append(
                        send(src, dst, t_s.at[number, kind], t_r.at[number, kind], (ep, t))
                    )
        if index >= 2:
            third(order[index - 2])
    sh_all[:, aligned(tp, sh_ref.shape[1])] = sh_ref[...]
    po_all[:, aligned(tp, po_ref.shape[1])] = po_ref[...]
    sq_all[tp] = sq_ref[...]
    for k in order[:-1]:
        z_copies[k].wait_recv()
        o_ref[...] += bz[k].astype(jnp.float32)
    for copy in t_copies:
        copy.wait()
    for group in (c_copies, dx_copies, dy_copies, x_copies, y_copies, z_copies):
        for copy in group.values():
            copy.wait_send()


def reduce_rows(hidden, down, shared_hidden, pooled, squares, n_ep, n_tp):
    n_z = n_ep // 2
    rows, width = hidden.shape[0] // n_ep, down.shape[1]
    cols = width // n_tp
    half = rows // 2
    bf16 = jnp.bfloat16
    vmem = pl.BlockSpec(memory_space=pltpu.VMEM)
    scratch = [
        pltpu.VMEM((n_z, 2 * rows, width), bf16),
        pltpu.VMEM((n_z, rows, width), bf16),
        pltpu.VMEM((n_z, rows, width), bf16),
        pltpu.VMEM((n_z, half, cols), bf16),
        pltpu.VMEM((n_z, half, cols), bf16),
        pltpu.VMEM((n_z, rows, cols), bf16),
        pltpu.VMEM((n_z, rows, cols), bf16),
        pltpu.VMEM((n_z, rows, cols), bf16),
        pltpu.VMEM((n_z, rows, cols), bf16),
    ]
    sems = [pltpu.SemaphoreType.DMA((n_z,))] * 12 + [pltpu.SemaphoreType.DMA((3, 3))] * 2
    return pl.pallas_call(
        lambda *refs: reduce_kernel(n_ep, *refs),
        out_shape=(
            jax.ShapeDtypeStruct((rows, cols), jnp.float32),
            jax.ShapeDtypeStruct((rows, n_tp * shared_hidden.shape[1]), bf16),
            jax.ShapeDtypeStruct((rows, n_tp * pooled.shape[1]), bf16),
            jax.ShapeDtypeStruct((n_tp,) + squares.shape, jnp.float32),
        ),
        in_specs=[vmem] * 5,
        out_specs=(vmem,) * 4,
        scratch_shapes=scratch + sems,
        compiler_params=pltpu.CompilerParams(
            collective_id=1, has_side_effects=True, vmem_limit_bytes=24 << 20
        ),
    )(hidden, down, shared_hidden, pooled, squares)


def dense_on_device(
    mix_input,
    expert_input,
    mix_gain,
    moe_gain,
    pool_in,
    pool_scale,
    pool_gain,
    pool_out,
    route,
    route_score,
    expert_gate,
    expert_up,
    expert_down,
    shared_gate,
    shared_up,
    shared_down,
):
    n_ep, n_tp = lax.axis_size("ep"), lax.axis_size("tp")
    me = lax.axis_index("ep")
    tok_rows = mix_input.shape[0]
    channels = pool_in.shape[1]
    pool_width = channels * n_tp
    f32 = jnp.float32

    moe_norm = row_norm(expert_input, moe_gain)
    weights = 2.5 * route_score / jnp.sum(route_score, axis=1, keepdims=True)
    experts = jnp.arange(n_ep, dtype=jnp.int32)
    dense = jnp.sum(
        jnp.where(route.T[None, :, :] == experts[:, None, None], weights.T[None, :, :], 0.0), axis=1
    )
    mix_norm = row_norm(mix_input, mix_gain)
    pool_input = jnp.dot(mix_norm, pool_in, preferred_element_type=f32).astype(jnp.bfloat16)
    before = shifted(pool_input[tok_rows - reach_rows :], "ep", 1)
    all_rows, all_weights, shared_hidden = gather_rows(
        moe_norm, dense, shared_gate, shared_up, n_ep
    )

    extended = jnp.concatenate([before, pool_input], axis=0).astype(f32)
    position = (me * tok_rows + jnp.arange(tok_rows, dtype=jnp.int32) + 1).astype(f32)
    channel_ids = lax.axis_index("tp") * channels + jnp.arange(channels, dtype=jnp.int32)
    group = channel_ids // (pool_width // 4)
    scaled = window_means(extended, position, group, tok_rows) * pool_scale
    squares = jnp.sum(scaled * scaled, axis=1)[None, :]
    pooled = (scaled * pool_gain).astype(jnp.bfloat16)
    factor = lax.dynamic_index_in_dim(all_weights, me, axis=1, keepdims=False).reshape(-1, 1)
    gate = jnp.dot(all_rows, expert_gate[0], preferred_element_type=f32)
    upper = jnp.dot(all_rows, expert_up[0], preferred_element_type=f32)
    hidden = (jax.nn.silu(gate) * upper * factor).astype(jnp.bfloat16)
    routed, shared_all, pooled_all, squares_all = reduce_rows(
        hidden, expert_down[0], shared_hidden, pooled, squares, n_ep, n_tp
    )
    mean = jnp.sum(squares_all, axis=0).reshape(-1, 1) / pool_width
    mix_out = (
        jnp.dot(pooled_all, pool_out, preferred_element_type=f32) * lax.rsqrt(mean + epsilon)
    ).astype(jnp.bfloat16)
    shared_part = jnp.dot(shared_all, shared_down, preferred_element_type=f32)
    return (mix_out, (routed + shared_part).astype(jnp.bfloat16))


def chosen(*arrays):
    route, expert_gate = arrays[8], arrays[10]
    experts = expert_gate.shape[0] * lax.axis_size("ep")
    capacity = 2 * route.shape[0] * route.shape[1] // experts
    square = lax.axis_size("tp") == 4 and lax.axis_size("ep") >= 6
    if capacity == route.shape[0] and expert_gate.shape[0] == 1 and square:
        return dense_on_device(*arrays)
    return on_device(*arrays)


def solution(mesh):
    return jax.shard_map(
        chosen,
        mesh=mesh,
        in_specs=(
            P("ep", None),
            P("ep", None),
            P(),
            P(),
            P(None, "tp"),
            P("tp"),
            P("tp"),
            P(None, "tp"),
            P("ep", None),
            P("ep", None),
            P("ep", None, "tp"),
            P("ep", None, "tp"),
            P("ep", "tp", None),
            P(None, "tp"),
            P(None, "tp"),
            P(None, "tp"),
        ),
        out_specs=(P("ep", "tp"), P("ep", "tp")),
        check_vma=False,
    )
```

profile of v0, /device:TPU:0, one launch (start us, length us, event | category | flops | bytes accessed | tf_op | source)
XLA Modules:
  0.0 92.0 jit_solution(5691516124526159760)
XLA Ops:
  0.6 0.0 copy-start
  0.6 0.0 copy-start.5
  0.7 0.0 copy-start.7
  0.7 0.0 copy-start.6
  0.7 0.0 copy-start.8
  0.7 1.4 %fusion.11 = f32[128]{0:T(128)S(1)} fusion(bf16[128,2048]{1,0:T(8,128)(2,1)} %param.16), kind=kLoop, calls=%fused_computation.17 | loop fusion | flops 786304 | bytes 524800 | tf_op jit(solution)/shard_map/reduce_sum | solution.py:21
  2.1 1.8 %convolution_convert_fusion = bf16[128,256]{1,0:T(8,128)(2,1)S(1)} fusion(bf16[2048,256]{1,0:T(8,128)(2,1)} %param.20, bf16[128,2048]{1,0:T(8,128)(2,1)} %param.16, f32[2048]{0:T(1024)} %param.18, f32[128]{0:T(128)S(1)} %add_rsqrt_fusion.1), kind=kOutput, calls=%fused_computation.13 | convolution fusion | flops 135299072 | bytes 1647104 | tf_op jit(solution)/shard_map/dot_general | solution.py:447
  3.9 2.4 %collective-permute-start = (bf16[15,256]{1,0:T(8,128)(2,1)S(1)}, bf16[15,256]{1,0:T(8,128)(2,1)S(1)}, u32[]{:S(2)}, u32[]{:S(2)}) collective-permute-start(bf16[15,256]{1,0:T(8,128)(2,1)S(1)} %slice.69), channel_id=1, source_target_pairs={{0,4},{4,8},{8,12},{12,16},{16,20},{20,24},{24,28},{1,5},{5,9},{9,... | collective-permute-start | bytes 23048 | tf_op jit(solution)/shard_map/ppermute | solution.py:16
  6.3 0.0 copy-done.5
  6.3 0.2 fusion.8
  6.5 0.0 copy-done.7
  6.6 0.0 copy-done.6
  6.6 0.2 fusion.10.refs_0_
  6.8 0.0 copy-done.8
  6.8 0.0 copy-start.2
  6.8 1.6 %copy-done.2 = bf16[2048,512]{1,0:T(8,128)(2,1)S(1)} copy-done((bf16[2048,512]{1,0:T(8,128)(2,1)S(1)}, bf16[2048,512]{1,0:T(8,128)(2,1)}, u32[]{:S(2)}) %copy-start.2) | copy-done | bytes 2097176
  8.4 0.0 copy-start.3
  8.4 1.6 %copy-done.3 = bf16[2048,512]{1,0:T(8,128)(2,1)S(1)} copy-done((bf16[2048,512]{1,0:T(8,128)(2,1)S(1)}, bf16[2048,512]{1,0:T(8,128)(2,1)}, u32[]{:S(2)}) %copy-start.3) | copy-done | bytes 2097176
  10.0 29.3 %shard_map.167 = (bf16[1024,2048]{1,0:T(8,128)(2,1)S(1)}, f32[8,8,128]{2,1,0:T(8,128)S(1)}, bf16[128,512]{1,0:T(8,128)(2,1)S(1)}) custom-call(bf16[128,2048]{1,0:T(8,128)(2,1)S(1)} %fusion.10.refs_0_, f32[8,128]{1,0:T(8,128)S(1)} %select_reduce_fusion.refs_1_, bf16[2048,512]{1,0:T(8,128)(2,1)S(1)} %copy-done.2, bf16[2048,512]{1,0:T(8,128)(2,1)S(1)} %copy-done.3), custom_call_target="tpu_custom_call" | custom-call | tf_op jit(solution)/shard_map/pallas_call | solution.py:244
  39.3 0.0 copy-start.4
  39.3 1.9 %copy-done.4 = bf16[1024,2048]{1,0:T(8,128)(2,1)} copy-done((bf16[1024,2048]{1,0:T(8,128)(2,1)}, bf16[1024,2048]{1,0:T(8,128)(2,1)S(1)}, u32[]{:S(2)}) %copy-start.4) | copy-done | bytes 4194328
  41.2 0.0 copy-done
  41.2 3.7 %fusion = f32[1024,512]{1,0:T(8,128)} fusion(bf16[1024,2048]{1,0:T(8,128)(2,1)S(1)} %get-tuple-element.9, bf16[1,2048,512]{2,1,0:T(8,128)(2,1)S(1)} %copy-done), kind=kOutput, calls=%fused_computation | convolution fusion | flops 2147483648 | bytes 8388608 | tf_op jit(solution)/shard_map/dot_general | solution.py:462
  44.9 0.0 copy-start.9
  44.9 6.1 %multiply_convert_fusion.refs_0_ = bf16[1024,512]{1,0:T(8,128)(2,1)S(1)} fusion(f32[1024,512]{1,0:T(8,128)} %fusion, bf16[1024,2048]{1,0:T(8,128)(2,1)} %copy-done.4, bf16[1,2048,512]{2,1,0:T(8,128)(2,1)} %param.26, f32[1024]{0:T(1024)S(1)} %bitcast.23), kind=kOutput, calls=%fused_computation.4 | convolution fusion | flops 2151153664 | bytes 9441280 | tf_op jit(solution)/shard_map/dot_general | solution.py:461
  51.0 0.0 copy-start.10
  51.0 0.0 copy-start.1
  51.1 0.0 collective-permute-done
  51.1 0.0 copy-done.9
  51.1 0.3 multiply_reduce_fusion
  51.4 0.3 copy-done.10
  51.7 0.9 copy-done.1
  52.6 34.4 %shard_map.168 = (f32[128,512]{1,0:T(8,128)S(1)}, bf16[128,2048]{1,0:T(8,128)(2,1)S(1)}, bf16[128,1024]{1,0:T(8,128)(2,1)S(1)}, f32[4,1,128]{2,1,0:T(1,128)S(1)}) custom-call(bf16[1024,512]{1,0:T(8,128)(2,1)S(1)} %multiply_convert_fusion.refs_0_, bf16[512,2048]{1,0:T(8,128)(2,1)S(1)} %bitcast.21, bf16[128,512]{1,0:T(8,128)(2,1)S(1)} %get-tuple-element.11.refs_2_, ...), custom_call_target="tpu_custom_call" | custom-call | tf_op jit(solution)/shard_map/pallas_call | solution.py:398
  87.1 2.2 %fusion.7 = bf16[128,512]{1,0:T(8,128)(2,1)} fusion(bf16[128,1024]{1,0:T(8,128)(2,1)S(1)} %get-tuple-element.12, bf16[1024,512]{1,0:T(8,128)(2,1)} %param.23, f32[128]{0:T(128)S(1)} %add_rsqrt_fusion), kind=kOutput, calls=%fused_computation.12 | convolution fusion | flops 134348800 | bytes 1442304 | tf_op jit(solution)/shard_map/dot_general | solution.py:469
  89.3 2.7 %fusion.6 = bf16[128,512]{1,0:T(8,128)(2,1)} fusion(f32[128,512]{1,0:T(8,128)S(1)} %get-tuple-element.14, bf16[128,2048]{1,0:T(8,128)(2,1)S(1)} %get-tuple-element.15, bf16[2048,512]{1,0:T(8,128)(2,1)} %param.31), kind=kOutput, calls=%fused_computation.11 | convolution fusion | flops 268566528 | bytes 3014656 | tf_op jit(solution)/shard_map/dot_general | solution.py:471
  (15 shorter events, 0.2 us)
Async XLA Ops:
  0.6 40.6 %copy-start = (bf16[1,2048,512]{2,1,0:T(8,128)(2,1)S(1)}, bf16[1,2048,512]{2,1,0:T(8,128)(2,1)}, u32[]{:S(2)}) copy-start(bf16[1,2048,512]{2,1,0:T(8,128)(2,1)} %param.27) | copy-start | bytes 6291460
  0.6 5.6 %copy-start.5 = (bf16[128,2048]{1,0:T(8,128)(2,1)S(1)}, bf16[128,2048]{1,0:T(8,128)(2,1)}, u32[]{:S(2)}) copy-start(bf16[128,2048]{1,0:T(8,128)(2,1)} %param.17) | copy-start | bytes 1572868
  0.7 5.8 %copy-start.7 = (f32[128,4]{0,1:T(4,128)S(1)}, f32[128,4]{0,1:T(4,128)}, u32[]{:S(2)}) copy-start(f32[128,4]{0,1:T(4,128)} %param.25) | copy-start | bytes 6148
  0.7 5.9 %copy-start.6 = (f32[2048]{0:T(1024)S(1)}, f32[2048]{0:T(1024)}, u32[]{:S(2)}) copy-start(f32[2048]{0:T(1024)} %param.19) | copy-start | bytes 24580
  0.7 6.1 %copy-start.8 = (s32[128,4]{0,1:T(4,128)S(1)}, s32[128,4]{0,1:T(4,128)}, u32[]{:S(2)}) copy-start(s32[128,4]{0,1:T(4,128)} %param.24) | copy-start | bytes 6148
  3.9 47.2 %collective-permute-start = (bf16[15,256]{1,0:T(8,128)(2,1)S(1)}, bf16[15,256]{1,0:T(8,128)(2,1)S(1)}, u32[]{:S(2)}, u32[]{:S(2)}) collective-permute-start(bf16[15,256]{1,0:T(8,128)(2,1)S(1)} %slice.69), channel_id=1, source_target_pairs={{0,4},{4,8},{8,12},{12,16},{16,20},{20,24},{24,28},{1,5},{5,9},{9,... | collective-permute-start | bytes 23048 | tf_op jit(solution)/shard_map/ppermute | solution.py:16
  6.8 1.6 %copy-start.2 = (bf16[2048,512]{1,0:T(8,128)(2,1)S(1)}, bf16[2048,512]{1,0:T(8,128)(2,1)}, u32[]{:S(2)}) copy-start(bf16[2048,512]{1,0:T(8,128)(2,1)} %refs_2_.1) | copy-start | bytes 6291460
  8.4 1.6 %copy-start.3 = (bf16[2048,512]{1,0:T(8,128)(2,1)S(1)}, bf16[2048,512]{1,0:T(8,128)(2,1)}, u32[]{:S(2)}) copy-start(bf16[2048,512]{1,0:T(8,128)(2,1)} %refs_3_.1) | copy-start | bytes 6291460
  39.3 1.9 %copy-start.4 = (bf16[1024,2048]{1,0:T(8,128)(2,1)}, bf16[1024,2048]{1,0:T(8,128)(2,1)S(1)}, u32[]{:S(2)}) copy-start(bf16[1024,2048]{1,0:T(8,128)(2,1)S(1)} %get-tuple-element.9) | copy-start | bytes 12582916
  44.9 6.2 %copy-start.9 = (f32[256]{0:T(256)S(1)}, f32[256]{0:T(256)}, u32[]{:S(2)}) copy-start(f32[256]{0:T(256)} %param.21) | copy-start | bytes 3076
  51.0 0.7 copy-start.10
  51.0 1.6 %copy-start.1 = (bf16[1,512,2048]{2,1,0:T(8,128)(2,1)S(1)}, bf16[1,512,2048]{2,1,0:T(8,128)(2,1)}, u32[]{:S(2)}) copy-start(bf16[1,512,2048]{2,1,0:T(8,128)(2,1)} %param.28) | copy-start | bytes 6291460
where the time goes:
time: 92.3 us; the launch traced here: 92 us
  Pallas kernels  63.7 us (69%)
  matrix products  16.4 us (18%)
  local copies, waits for them, and re-layouts  6.34 us (7%)
  starting transfers between devices  2.4 us (3%)
  other arithmetic  2.24 us (2%)
    pallas_call x1, Pallas kernels, reduce_rows(): pl.pallas_call(lambda *refs: reduce_kernel(n_ep, *refs), out_shape=(jax.S...  34.4 us
    pallas_call x1, Pallas kernels, gather_rows(): pl.pallas_call(lambda *refs: gather_kernel(n_ep, *refs), out_shape=(jax.S...  29.3 us
    unnamed x22, local copies, waits for them, and re-layouts  6.32 us
    dot_general x1, matrix products, dense_on_device(): gate = jnp.dot(all_rows, expert_gate[0], preferred_element_type=f32)  6.11 us
    dot_general x1, matrix products, dense_on_device(): upper = jnp.dot(all_rows, expert_up[0], preferred_element_type=f32)  3.66 us
    dot_general x1, matrix products, dense_on_device(): shared_part = jnp.dot(shared_all, shared_down, preferred_element_type=f32)  2.7 us
    ppermute x1, starting transfers between devices, shifted(): return lax.ppermute(block, axis, route)  2.4 us
    dot_general x1, matrix products, dense_on_device(): jnp.dot(pooled_all, pool_out, preferred_element_type=f32)  2.2 us
  transfers between devices with their start and end apart: 1, of which 0 were waited for; matrix products, arithmetic and copies ran while one was open for 11% of the time, Pallas kernels for 32%

commit v1 on v0

v1 whole, which is shorter than its diff:
```python
import jax
import jax.numpy as jnp
from jax import lax
from jax.experimental import pallas as pl
from jax.experimental.pallas import tpu as pltpu
from jax.sharding import PartitionSpec as P

epsilon = 1e-06
reach_rows = 15
window_widths = (2, 4, 8, 16)


def shifted(block, axis, distance):
    devices = range(lax.axis_size(axis))
    route = [(i - distance, i) for i in devices if i - distance in devices]
    return lax.ppermute(block, axis, route)


def row_norm(rows, gain):
    values = rows.astype(jnp.float32)
    scale = lax.rsqrt(jnp.mean(values * values, axis=-1, keepdims=True) + epsilon)
    return (values * scale * gain).astype(jnp.bfloat16)


def window_means(extended, position, group, n_rows):
    total = jnp.zeros((n_rows, extended.shape[1]), jnp.float32)
    result = jnp.zeros((n_rows, extended.shape[1]), jnp.float32)
    for lag in range(16):
        total = total + extended[reach_rows - lag : reach_rows - lag + n_rows]
        for index, width in enumerate(window_widths):
            if lag + 1 == width:
                count = jnp.minimum(position, float(width))[:, None]
                result = jnp.where(group[None, :] == index, total / count, result)
    return result - extended[reach_rows:]


def serve(sending, expert_gate, expert_up, expert_down):
    arrived = lax.all_to_all(sending, "ep", split_axis=0, concat_axis=0, tiled=True)
    gate = jnp.einsum("send,edf->senf", arrived, expert_gate, preferred_element_type=jnp.float32)
    upper = jnp.einsum("send,edf->senf", arrived, expert_up, preferred_element_type=jnp.float32)
    hidden = (jax.nn.silu(gate) * upper).astype(jnp.bfloat16)
    term = jnp.einsum("senf,efd->send", hidden, expert_down, preferred_element_type=jnp.float32)
    summed = lax.psum_scatter(term.astype(jnp.bfloat16), "tp", scatter_dimension=3, tiled=True)
    return lax.all_to_all(summed, "ep", split_axis=0, concat_axis=0, tiled=True)


def on_device(
    mix_input,
    expert_input,
    mix_gain,
    moe_gain,
    pool_in,
    pool_scale,
    pool_gain,
    pool_out,
    route,
    route_score,
    expert_gate,
    expert_up,
    expert_down,
    shared_gate,
    shared_up,
    shared_down,
):
    tok_rows = mix_input.shape[0]
    channels = pool_in.shape[1]
    pool_width = channels * lax.axis_size("tp")
    mix_norm = row_norm(mix_input, mix_gain)
    pool_input = jnp.dot(mix_norm, pool_in, preferred_element_type=jnp.float32).astype(jnp.bfloat16)
    before = shifted(pool_input[tok_rows - reach_rows :], "ep", 1)
    extended = jnp.concatenate([before, pool_input], axis=0).astype(jnp.float32)
    position = (lax.axis_index("ep") * tok_rows + jnp.arange(tok_rows, dtype=jnp.int32) + 1).astype(
        jnp.float32
    )
    channel_ids = lax.axis_index("tp") * channels + jnp.arange(channels, dtype=jnp.int32)
    group = channel_ids // (pool_width // 4)
    scaled = window_means(extended, position, group, tok_rows) * pool_scale
    squares = lax.psum(jnp.sum(scaled * scaled, axis=1), "tp")
    pooled_norm = (scaled * lax.rsqrt(squares / pool_width + epsilon)[:, None] * pool_gain).astype(
        jnp.bfloat16
    )
    moe_norm = row_norm(expert_input, moe_gain)
    shared_hidden = (
        jax.nn.silu(jnp.dot(moe_norm, shared_gate, preferred_element_type=jnp.float32))
        * jnp.dot(moe_norm, shared_up, preferred_element_type=jnp.float32)
    ).astype(jnp.bfloat16)
    pooled_all, shared_all = (
        lax.all_gather(pooled_norm, "tp", axis=1, tiled=True),
        lax.all_gather(shared_hidden, "tp", axis=1, tiled=True),
    )
    mix_out = jnp.dot(pooled_all, pool_out, preferred_element_type=jnp.float32).astype(jnp.bfloat16)
    shared_part = jnp.dot(shared_all, shared_down, preferred_element_type=jnp.float32)
    n_tok, top = route.shape
    local_experts = expert_gate.shape[0]
    experts = local_experts * lax.axis_size("ep")
    capacity = 2 * n_tok * top // experts
    flat_route = route.reshape(-1)
    table = (flat_route[:, None] == jnp.arange(experts, dtype=jnp.int32)[None, :]).astype(jnp.int32)
    ranks = jnp.sum((jnp.cumsum(table, axis=0) - table) * table, axis=1)
    slot = flat_route * capacity + ranks
    owner = (
        jnp.full((experts * capacity,), n_tok, jnp.int32)
        .at[slot]
        .set(jnp.arange(n_tok * top, dtype=jnp.int32) // top)
    )
    padded_rows = jnp.concatenate(
        [moe_norm, jnp.zeros((1, moe_norm.shape[1]), jnp.bfloat16)], axis=0
    )
    outgoing = padded_rows[owner].reshape(
        lax.axis_size("ep"), local_experts, capacity, moe_norm.shape[1]
    )
    middle = capacity // 2
    first = serve(outgoing[:, :, :middle], expert_gate, expert_up, expert_down)
    second = serve(outgoing[:, :, middle:], expert_gate, expert_up, expert_down)
    returned = jnp.concatenate([first, second], axis=2)
    back_rows = returned.reshape(experts * capacity, returned.shape[3])
    picked = back_rows[slot].reshape(n_tok, top, returned.shape[3]).astype(jnp.float32)
    weights = 2.5 * route_score / jnp.sum(route_score, axis=1, keepdims=True)
    routed = jnp.sum(picked * weights[:, :, None], axis=1)
    moe_out = (routed + shared_part).astype(jnp.bfloat16)
    return (mix_out, moe_out)


MESH = pl.DeviceIdType.MESH


def places():
    ep, tp = lax.axis_index("ep"), lax.axis_index("tp")
    z, core = ep // 2, ep % 2
    y, x = tp // 2, tp % 2
    return ep, tp, z, core, y * 2 + 1 - x, (1 - y) * 2 + x, (1 - y) * 2 + 1 - x


def greet(partners):
    barrier = pltpu.get_barrier_semaphore()
    for partner in partners:
        pl.semaphore_signal(barrier, inc=1, device_id=partner, device_id_type=MESH)
    pl.semaphore_wait(barrier, len(partners))


def aligned(start, size):
    return pl.ds(pl.multiple_of(start * size, size), size)


def fused_kernel(n_ep, n_tp, *refs):
    hbm, (mix_ref, moe_ref), rest = refs[:16], refs[16:18], refs[18:]
    (mi_h, ei_h, mg_h, eg_h, pi_h, ps_h, pg_h, po_h, rt_h, sc_h, wg_h, wu_h, wd_h, sg_h, su_h, sd_h) = hbm
    staged, rest = rest[:16], rest[16:]
    (mi, ei, mg, eg, pin, pscale, pgain, pout, rt, sc, wg, wu, wd, sg, su, sd) = staged
    (g, dense, mm, halo_s, halo_r, ext, sh_all, po_all, sq_all, hid) = rest[:10]
    (p, ca, s, bx, by, qx, qy, r, bz, o) = rest[10:20]
    l_sem = rest[20]
    (w_s, w_r, z_s, z_r, gx_s, gx_r, gy_s, gy_r, gu_s, gu_r, gv_s, gv_r, gc_s, gc_r) = rest[21:35]
    (c_s, c_r, dx_s, dx_r, dy_s, dy_r, x_s, x_r, y_s, y_r, f_s, f_r, t_s, t_r, q_s, q_r, h_s, h_r) = rest[35:]
    ep, tp, z, core, xn, yn, dg = places()
    n_z = n_ep // 2
    rows, width = ei.shape
    cols = width // n_tp
    half = rows // 2
    f32, bf16 = jnp.float32, jnp.bfloat16
    other_core = z * 2 + 1 - core
    own_rows = aligned(ep, rows)
    low, high = pl.ds(0, half), pl.ds(half, half)

    loads = {}
    for number in (8, 9, 1, 3, 0, 2, 4, 13, 14, 5, 6, 10, 11, 12, 15, 7):
        loads[number] = pltpu.make_async_copy(hbm[number], staged[number], l_sem.at[number])
        loads[number].start()

    def send(src, dst, sem_s, sem_r, device):
        copy = pltpu.make_async_remote_copy(
            src_ref=src, dst_ref=dst, send_sem=sem_s, recv_sem=sem_r, device_id=device, device_id_type=MESH
        )
        copy.start()
        return copy

    peers = (xn, yn, dg)
    partners = [((ep + m) % n_ep, tp) for m in range(1, n_ep)] + [(ep, t) for t in peers]
    barrier = pltpu.get_barrier_semaphore()
    for partner in partners:
        pl.semaphore_signal(barrier, inc=1, device_id=partner, device_id_type=MESH)

    def norm_into(src, gain, dst, start):
        step = 16

        def some(index, carry):
            values = src[aligned(index, step), :].astype(f32)
            scale = lax.rsqrt(jnp.mean(values * values, axis=-1, keepdims=True) + epsilon)
            dst[pl.ds(pl.multiple_of(start + index * step, step), step), :] = (
                values * scale * gain[...]
            ).astype(bf16)
            return carry

        lax.fori_loop(0, rows // step, some, 0)

    with jax.named_scope("norm"):
        loads[8].wait()
        loads[9].wait()
        total_score = jnp.sum(sc[...], axis=0, keepdims=True)
        expert_ids = lax.broadcasted_iota(jnp.int32, (n_ep, rows), 0)
        mine = jnp.zeros((n_ep, rows), f32)
        for choice in range(rt.shape[0]):
            share = 2.5 * sc[choice : choice + 1, :] / total_score
            mine = mine + jnp.where(rt[choice : choice + 1, :] == expert_ids, share, 0.0)
        dense[ep] = mine
        loads[1].wait()
        loads[3].wait()
        norm_into(ei, eg, g, ep * rows)
    with jax.named_scope("greet"):
        pl.semaphore_wait(barrier, len(partners))
    w_copies = [
        send(dense.at[ep], dense.at[ep], w_s.at[m], w_r.at[m], ((ep + m) % n_ep, tp))
        for m in range(1, n_ep)
    ]
    order = [1, n_z - 1] + list(range(2, n_z - 1))
    z_copies, gx, gy, gu, gv, gc = {}, {}, {}, {}, {}, {}
    for k in order:
        piece = g.at[own_rows, aligned(tp, cols)]
        z_copies[k] = send(piece, piece, z_s.at[k], z_r.at[k], (((z + k) % n_z) * 2 + core, tp))
    whole = g.at[own_rows, :]
    gc[0] = send(whole, whole, gc_s.at[0], gc_r.at[0], (other_core, tp))

    with jax.named_scope("shared"):
        loads[13].wait()
        loads[14].wait()
        fs = sg.shape[1]
        tile = 256

        def shared_tile(index, carry):
            part = aligned(index, tile)
            gate = jnp.dot(g[own_rows, :], sg[:, part], preferred_element_type=f32)
            upper = jnp.dot(g[own_rows, :], su[:, part], preferred_element_type=f32)
            sh_all[:, pl.ds(pl.multiple_of(tp * fs + index * tile, tile), tile)] = (
                gate / (1.0 + jnp.exp(-gate)) * upper
            ).astype(bf16)
            return carry

        lax.fori_loop(0, fs // tile, shared_tile, 0)
    t_copies = {}

    def spread(kind, buffer):
        size = buffer.shape[1] // n_tp
        mine_slot = buffer.at[:, aligned(tp, size)]
        t_copies[kind, 0] = send(mine_slot, mine_slot, t_s.at[kind, 0], t_r.at[kind, 0], (ep, xn))
        t_copies[kind, 1] = send(mine_slot, mine_slot, t_s.at[kind, 1], t_r.at[kind, 1], (ep, yn))

    def spread_corner(kind, buffer):
        size = buffer.shape[1] // n_tp
        t_copies[kind, 0].wait_recv()
        part = buffer.at[low, aligned(xn, size)]
        t_copies[kind, 2] = send(part, part, t_s.at[kind, 2], t_r.at[kind, 2], (ep, yn))
        t_copies[kind, 1].wait_recv()
        part = buffer.at[high, aligned(yn, size)]
        t_copies[kind, 3] = send(part, part, t_s.at[kind, 3], t_r.at[kind, 3], (ep, xn))

    spread(0, sh_all)

    channels = pin.shape[1]
    reach = halo_s.shape[0]
    with jax.named_scope("pool_in"):
        loads[0].wait()
        loads[2].wait()
        norm_into(mi, mg, mm, 0)
        loads[4].wait()
        pooled_in = jnp.dot(mm[...], pin[...], preferred_element_type=f32).astype(bf16)
        halo_s[...] = pooled_in[rows - reach :]
        ext[reach:, :] = pooled_in.astype(f32)
        halo = send(halo_s, halo_r, h_s, h_r, ((ep + 1) % n_ep, tp))

    eye = lax.broadcasted_iota(jnp.int32, (rows, rows), 0) == lax.broadcasted_iota(
        jnp.int32, (rows, rows), 1
    )

    def window():
        halo.wait_recv()
        ext[:reach, :] = jnp.where(ep == 0, 0.0, halo_r[...].astype(f32))
        position = (ep * rows + 1 + lax.broadcasted_iota(jnp.int32, (rows, 1), 0)).astype(f32)
        total = jnp.zeros((rows, channels), f32)
        result = jnp.zeros((rows, channels), f32)
        for lag in range(reach):
            total = total + ext[reach - lag : reach - lag + rows, :]
            for index, size in enumerate(window_widths):
                if lag + 1 == size:
                    count = jnp.minimum(position, float(size))
                    result = jnp.where(tp == index, total / count, result)
        loads[5].wait()
        loads[6].wait()
        scaled = (result - ext[reach:, :]) * pscale[...]
        squares = jnp.sum(scaled * scaled, axis=1, keepdims=True)
        sq_all[tp] = jnp.sum(jnp.where(eye, squares, 0.0), axis=0, keepdims=True)
        po_all[:, aligned(tp, channels)] = (scaled * pgain[...]).astype(bf16)

    def block(k):
        return ((z + n_z - k) % n_z) * 2 + core

    def gathered(k, quarter):
        return g.at[aligned(block(k), rows), aligned(quarter, cols)]

    def gathered_half(k, part, quarter):
        start = pl.multiple_of(block(k) * rows + part * half, half)
        return g.at[pl.ds(start, half), aligned(quarter, cols)]

    def across(k):
        with jax.named_scope(f"across{k}"):
            z_copies[k].wait_recv()
            part = gathered(k, tp)
            gx[k] = send(part, part, gx_s.at[k], gx_r.at[k], (ep, xn))
            gy[k] = send(part, part, gy_s.at[k], gy_r.at[k], (ep, yn))

    def corner(k):
        with jax.named_scope(f"corner{k}"):
            gx[k].wait_recv()
            part = gathered_half(k, 0, xn)
            gu[k] = send(part, part, gu_s.at[k], gu_r.at[k], (ep, yn))
            gy[k].wait_recv()
            part = gathered_half(k, 1, yn)
            gv[k] = send(part, part, gv_s.at[k], gv_r.at[k], (ep, xn))

    def over(k):
        with jax.named_scope(f"over{k}"):
            gu[k].wait_recv()
            gv[k].wait_recv()
            part = g.at[aligned(block(k), rows), :]
            gc[k] = send(part, part, gc_s.at[k], gc_r.at[k], (other_core, tp))

    c_copies, dx_copies, dy_copies, x_copies, y_copies, f_copies = {}, {}, {}, {}, {}, {}
    fe = wg.shape[1]

    def compute(k):
        plane = (z + n_z - k) % n_z
        with jax.named_scope(f"wait_over{k}"):
            gc[k].wait_recv()
        with jax.named_scope(f"hidden{k}"):
            pair = aligned(plane, 2 * rows)
            factors = []
            for part in range(2):
                line = dense[plane * 2 + part, pl.ds(ep, 1), :]
                factors.append(jnp.sum(jnp.where(eye, line, 0.0), axis=1, keepdims=True))
            factor = jnp.concatenate(factors, axis=0)

            def tile_hidden(index, carry):
                part = aligned(index, tile)
                gate = jnp.dot(g[pair, :], wg[:, part], preferred_element_type=f32)
                upper = jnp.dot(g[pair, :], wu[:, part], preferred_element_type=f32)
                hid[:, part] = (gate / (1.0 + jnp.exp(-gate)) * upper * factor).astype(bf16)
                return carry

            lax.fori_loop(0, fe // tile, tile_hidden, 0)
        with jax.named_scope(f"down{k}"):

            def tile_down(index, carry):
                part = aligned(index, cols)
                p[k, :, part] = jnp.dot(hid[...], wd[:, part], preferred_element_type=f32).astype(bf16)
                return carry

            lax.fori_loop(0, width // cols, tile_down, 0)
            c_copies[k] = send(
                p.at[k, aligned(1 - core, rows), :], ca.at[k], c_s.at[k], c_r.at[k], (other_core, tp)
            )

    def first(k):
        with jax.named_scope(f"first{k}"):
            c_copies[k].wait_recv()
            s[k] = (p[k, aligned(core, rows), :].astype(f32) + ca[k].astype(f32)).astype(bf16)
            dx_copies[k] = send(
                s.at[k, low, aligned(dg, cols)], bx.at[k], dx_s.at[k], dx_r.at[k], (ep, xn)
            )
            dy_copies[k] = send(
                s.at[k, high, aligned(dg, cols)], by.at[k], dy_s.at[k], dy_r.at[k], (ep, yn)
            )

    def second(k):
        with jax.named_scope(f"second{k}"):
            dx_copies[k].wait_recv()
            s[k, low, aligned(yn, cols)] = (
                s[k, low, aligned(yn, cols)].astype(f32) + bx[k].astype(f32)
            ).astype(bf16)
            y_copies[k] = send(
                s.at[k, :, aligned(yn, cols)], qy.at[k], y_s.at[k], y_r.at[k], (ep, yn)
            )
            dy_copies[k].wait_recv()
            s[k, high, aligned(xn, cols)] = (
                s[k, high, aligned(xn, cols)].astype(f32) + by[k].astype(f32)
            ).astype(bf16)
            x_copies[k] = send(
                s.at[k, :, aligned(xn, cols)], qx.at[k], x_s.at[k], x_r.at[k], (ep, xn)
            )

    def third(k):
        with jax.named_scope(f"third{k}"):
            x_copies[k].wait_recv()
            y_copies[k].wait_recv()
            total = (
                s[k, :, aligned(tp, cols)].astype(f32) + qx[k].astype(f32) + qy[k].astype(f32)
            )
            if k == 0:
                o[...] += total
            else:
                r[k] = total.astype(bf16)
                f_copies[k] = send(
                    r.at[k], bz.at[k], f_s.at[k], f_r.at[k], (((z + n_z - k) % n_z) * 2 + core, tp)
                )

    q_copies = []

    def finish_t():
        with jax.named_scope("epilogue"):
            for kind in range(2):
                t_copies[kind, 2].wait_recv()
                t_copies[kind, 3].wait_recv()
            for copy in q_copies:
                copy.wait()
            loads[15].wait()
            loads[7].wait()
            o[...] = jnp.dot(sh_all[...], sd[...], preferred_element_type=f32)
            mean = jnp.sum(sq_all[...], axis=0) / (channels * n_tp)
            inverse = lax.rsqrt(mean + epsilon)
            inverse = jnp.sum(jnp.where(eye, inverse, 0.0), axis=1, keepdims=True)
            mix_ref[...] = (
                jnp.dot(po_all[...], pout[...], preferred_element_type=f32) * inverse
            ).astype(bf16)

    with jax.named_scope("w_wait"):
        for copy in w_copies:
            copy.wait()
    with jax.named_scope("weights_wait"):
        for number in (10, 11, 12):
            loads[number].wait()
    with jax.named_scope("window"):
        window()
        spread(1, po_all)
        for number, t in enumerate(peers):
            q_copies.append(send(sq_all.at[tp], sq_all.at[tp], q_s.at[number], q_r.at[number], (ep, t)))

    far = order[2:]
    compute(0)
    across(order[0])
    across(order[1])
    with jax.named_scope("spread_corner"):
        spread_corner(0, sh_all)
        spread_corner(1, po_all)
    first(0)
    for k in far:
        across(k)
    corner(order[0])
    corner(order[1])
    over(order[0])
    over(order[1])
    second(0)
    for k in far:
        corner(k)
    finish_t()
    compute(order[0])
    for k in far:
        over(k)
    first(order[0])
    compute(order[1])
    third(0)
    second(order[0])
    first(order[1])
    todo = order[1:]
    for k in far:
        compute(k)
        second(todo[0])
        first(k)
        third(order[order.index(todo[0]) - 1])
        todo = todo[1:]
    second(order[-1])
    third(order[-2])
    third(order[-1])
    with jax.named_scope("final"):
        for k in order[:-1]:
            f_copies[k].wait_recv()
            o[...] += bz[k].astype(f32)
        f_copies[order[-1]].wait_recv()
        moe_ref[...] = (o[...] + bz[order[-1]].astype(f32)).astype(bf16)
    with jax.named_scope("drain"):
        halo.wait_send()
        for group in (
            z_copies, gx, gy, gu, gv, gc, t_copies,
            c_copies, dx_copies, dy_copies, x_copies, y_copies, f_copies,
        ):
            for copy in group.values():
                copy.wait_send()


def dense_on_device(
    mix_input,
    expert_input,
    mix_gain,
    moe_gain,
    pool_in,
    pool_scale,
    pool_gain,
    pool_out,
    route,
    route_score,
    expert_gate,
    expert_up,
    expert_down,
    shared_gate,
    shared_up,
    shared_down,
):
    n_ep, n_tp = lax.axis_size("ep"), lax.axis_size("tp")
    n_z = n_ep // 2
    operands = (
        mix_input,
        expert_input,
        mix_gain.reshape(1, -1),
        moe_gain.reshape(1, -1),
        pool_in,
        pool_scale.reshape(1, -1),
        pool_gain.reshape(1, -1),
        pool_out,
        route.T,
        route_score.T,
        expert_gate[0],
        expert_up[0],
        expert_down[0],
        shared_gate,
        shared_up,
        shared_down,
    )
    rows, width = expert_input.shape
    cols = width // n_tp
    half = rows // 2
    channels = pool_in.shape[1]
    reach = reach_rows + 1
    f32, bf16 = jnp.float32, jnp.bfloat16
    scratch = [pltpu.VMEM(a.shape, a.dtype) for a in operands] + [
        pltpu.VMEM((n_ep * rows, width), bf16),
        pltpu.VMEM((n_ep, n_ep, rows), f32),
        pltpu.VMEM((rows, width), bf16),
        pltpu.VMEM((reach, channels), bf16),
        pltpu.VMEM((reach, channels), bf16),
        pltpu.VMEM((reach + rows, channels), f32),
        pltpu.VMEM((rows, n_tp * shared_gate.shape[1]), bf16),
        pltpu.VMEM((rows, n_tp * channels), bf16),
        pltpu.VMEM((n_tp, 1, rows), f32),
        pltpu.VMEM((2 * rows, expert_gate.shape[2]), bf16),
        pltpu.VMEM((n_z, 2 * rows, width), bf16),
        pltpu.VMEM((n_z, rows, width), bf16),
        pltpu.VMEM((n_z, rows, width), bf16),
        pltpu.VMEM((n_z, half, cols), bf16),
        pltpu.VMEM((n_z, half, cols), bf16),
        pltpu.VMEM((n_z, rows, cols), bf16),
        pltpu.VMEM((n_z, rows, cols), bf16),
        pltpu.VMEM((n_z, rows, cols), bf16),
        pltpu.VMEM((n_z, rows, cols), bf16),
        pltpu.VMEM((rows, cols), f32),
    ]
    dma = pltpu.SemaphoreType.DMA
    sems = (
        [dma((len(operands),))]
        + [dma((n_ep,))] * 2
        + [dma((n_z,))] * 24
        + [dma((2, 4))] * 2
        + [dma((3,))] * 2
        + [dma] * 2
    )
    return pl.pallas_call(
        lambda *refs: fused_kernel(n_ep, n_tp, *refs),
        out_shape=(
            jax.ShapeDtypeStruct((rows, cols), bf16),
            jax.ShapeDtypeStruct((rows, cols), bf16),
        ),
        in_specs=[pl.BlockSpec(memory_space=pltpu.HBM)] * len(operands),
        out_specs=(pl.BlockSpec(memory_space=pltpu.VMEM),) * 2,
        scratch_shapes=scratch + sems,
        compiler_params=pltpu.CompilerParams(
            collective_id=0, has_side_effects=True, vmem_limit_bytes=60 << 20
        ),
        name="fused",
    )(*operands)


def chosen(*arrays):
    route, expert_gate = arrays[8], arrays[10]
    experts = expert_gate.shape[0] * lax.axis_size("ep")
    capacity = 2 * route.shape[0] * route.shape[1] // experts
    square = lax.axis_size("tp") == 4 and lax.axis_size("ep") >= 6
    if capacity == route.shape[0] and expert_gate.shape[0] == 1 and square:
        return dense_on_device(*arrays)
    return on_device(*arrays)


def solution(mesh):
    return jax.shard_map(
        chosen,
        mesh=mesh,
        in_specs=(
            P("ep", None),
            P("ep", None),
            P(),
            P(),
            P(None, "tp"),
            P("tp"),
            P("tp"),
            P(None, "tp"),
            P("ep", None),
            P("ep", None),
            P("ep", None, "tp"),
            P("ep", None, "tp"),
            P("ep", "tp", None),
            P(None, "tp"),
            P(None, "tp"),
            P(None, "tp"),
        ),
        out_specs=(P("ep", "tp"), P("ep", "tp")),
        check_vma=False,
    )
```

time: 92.3 us -> 72 us (0.78)
  matrix products: 16.4 us -> 0 us
  Pallas kernels: 63.7 us -> 68 us
  local copies, waits for them, and re-layouts: 6.34 us -> 3.14 us
  starting transfers between devices: 2.4 us -> 0 us
  other arithmetic: 2.24 us -> 0 us
    dot_general x5 -> x0, matrix products: 16.4 us -> none  [the longest x1 6.11 us: dense_on_device(): gate = jnp.dot(all_rows, expert_gate[0], preferred_element_type=f32)]
    pallas_call x2 -> x1, Pallas kernels: 63.7 us -> 68 us  [dense_on_device(): pl.pallas_call(lambda *refs: fused_kernel(n_ep, n_tp, *refs), out_shape=(...]
    unnamed x22 -> x2, local copies, waits for them, and re-layouts: 6.32 us -> 3.14 us
    ppermute x1 -> x0, starting transfers between devices: 2.4 us -> none  [shifted(): return lax.ppermute(block, axis, route)]
    reduce_sum x6 -> x0, other arithmetic: 1.94 us -> none  [the longest x2 1.57 us: row_norm(): jnp.mean(values * values, axis=-1, keepdims=True) + epsilon]
  transfers between devices with their start and end apart: 1 -> 0, of which waited for: 0 -> 0; matrix products, arithmetic and copies ran while one was open for 11% -> 0% of each run, Pallas kernels for 32% -> 0%
where the time goes in v1:
time: 72 us; the launch traced here: 71.8 us
  Pallas kernels  68 us (94%)
  local copies, waits for them, and re-layouts  3.14 us (4%)
    pallas_call x1, Pallas kernels, dense_on_device(): pl.pallas_call(lambda *refs: fused_kernel(n_ep, n_tp, *refs), out_shape=(...  68 us
    unnamed x2, local copies, waits for them, and re-layouts  3.14 us

profile of v1, /device:TPU:0, one launch (start us, length us, event | category | flops | bytes accessed | tf_op | source)
XLA Modules:
  0.0 71.8 jit_solution(14074764474112406327)
XLA Ops:
  0.6 68.0 %fused.1 = (bf16[128,512]{1,0:T(8,128)(2,1)}, bf16[128,512]{1,0:T(8,128)(2,1)}) custom-call(bf16[128,2048]{1,0:T(8,128)(2,1)} %refs_0_.1, bf16[128,2048]{1,0:T(8,128)(2,1)} %refs_1_.1, f32[1,2048]{1,0:T(1,128)} %bitcast.12, f32[1,2048]{1,0:T(1,128)} %bitcast.13, bf16[2048,256]{1,0:T(8,128)(2,1)} %refs_4_.1, f32[1,256]{1,0:T(1,128)} %bitcast.16, ...), custom_call_target="tpu_custom_call" | custom-call | tf_op jit(solution)/shard_map/fused/pallas_call | solution.py:562
  68.7 1.6 %copy.20 = bf16[128,512]{1,0:T(8,128)(2,1)} copy(bf16[128,512]{1,0:T(8,128)(2,1)} %get-tuple-element.4) | data formatting | bytes 262144
  70.2 1.6 %copy.21 = bf16[128,512]{1,0:T(8,128)(2,1)} copy(bf16[128,512]{1,0:T(8,128)(2,1)} %get-tuple-element.5) | data formatting | bytes 262144

commit v2 on v1

--- a/solution.py
+++ b/solution.py
@@ -131,13 +131,6 @@
     return ep, tp, z, core, y * 2 + 1 - x, (1 - y) * 2 + x, (1 - y) * 2 + 1 - x
 
 
-def greet(partners):
-    barrier = pltpu.get_barrier_semaphore()
-    for partner in partners:
-        pl.semaphore_signal(barrier, inc=1, device_id=partner, device_id_type=MESH)
-    pl.semaphore_wait(barrier, len(partners))
-
-
 def aligned(start, size):
     return pl.ds(pl.multiple_of(start * size, size), size)
 
@@ -148,10 +141,10 @@
     staged, rest = rest[:16], rest[16:]
     (mi, ei, mg, eg, pin, pscale, pgain, pout, rt, sc, wg, wu, wd, sg, su, sd) = staged
     (g, dense, mm, halo_s, halo_r, ext, sh_all, po_all, sq_all, hid) = rest[:10]
-    (p, ca, s, bx, by, qx, qy, r, bz, o) = rest[10:20]
-    l_sem = rest[20]
-    (w_s, w_r, z_s, z_r, gx_s, gx_r, gy_s, gy_r, gu_s, gu_r, gv_s, gv_r, gc_s, gc_r) = rest[21:35]
-    (c_s, c_r, dx_s, dx_r, dy_s, dy_r, x_s, x_r, y_s, y_r, f_s, f_r, t_s, t_r, q_s, q_r, h_s, h_r) = rest[35:]
+    (p, ca, s, bx, by, qx, qy, r, bz, o, so) = rest[10:21]
+    l_sem = rest[21]
+    (w_s, w_r, zu_s, zd_s, zf_s, z_r, e_s, e_r, d_s, d_r, gc_s, gc_r) = rest[22:34]
+    (c_s, c_r, dx_s, dx_r, dy_s, dy_r, x_s, x_r, y_s, y_r, f_s, f_r, t_s, t_r, q_s, q_r, h_s, h_r) = rest[34:]
     ep, tp, z, core, xn, yn, dg = places()
     n_z = n_ep // 2
     rows, width = ei.shape
@@ -174,6 +167,15 @@
         copy.start()
         return copy
 
+    halo = pltpu.make_async_remote_copy(
+        src_ref=halo_s,
+        dst_ref=halo_r,
+        send_sem=h_s,
+        recv_sem=h_r,
+        device_id=((ep + 1) % n_ep, tp),
+        device_id_type=MESH,
+    )
+    halo_r[...] = jnp.zeros_like(halo_r)
     peers = (xn, yn, dg)
     partners = [((ep + m) % n_ep, tp) for m in range(1, n_ep)] + [(ep, t) for t in peers]
     barrier = pltpu.get_barrier_semaphore()
@@ -208,17 +210,88 @@
         norm_into(ei, eg, g, ep * rows)
     with jax.named_scope("greet"):
         pl.semaphore_wait(barrier, len(partners))
-    w_copies = [
-        send(dense.at[ep], dense.at[ep], w_s.at[m], w_r.at[m], ((ep + m) % n_ep, tp))
-        for m in range(1, n_ep)
-    ]
-    order = [1, n_z - 1] + list(range(2, n_z - 1))
-    z_copies, gx, gy, gu, gv, gc = {}, {}, {}, {}, {}, {}
-    for k in order:
-        piece = g.at[own_rows, aligned(tp, cols)]
-        z_copies[k] = send(piece, piece, z_s.at[k], z_r.at[k], (((z + k) % n_z) * 2 + core, tp))
+    w_copies = {}
+    for m in range(1, n_ep):
+        target = ((z + m // 2) % n_z) * 2 + (core + m) % 2
+        w_copies[m] = send(dense.at[ep], dense.at[ep], w_s.at[m], w_r.at[ep], (target, tp))
+
+    side = jnp.where(core == 0, tp % 2, tp // 2)
+    facing = jnp.where(core == 0, xn, yn)
+    wide = width // 2
+
+    def z_piece(plane, part, columns):
+        start = pl.multiple_of((plane * 2 + core) * rows + part * half, half)
+        return g.at[pl.ds(start, half), aligned(columns, wide)]
+
+    def remote(piece, sem_s, sem_r, device):
+        return pltpu.make_async_remote_copy(
+            src_ref=piece, dst_ref=piece, send_sem=sem_s, recv_sem=sem_r, device_id=device, device_id_type=MESH
+        )
+
+    upper_z, lower_z = jnp.minimum(z + 1, n_z - 1), jnp.maximum(z - 1, 0)
+    for part in range(2):
+        piece = z_piece(z, part, side)
+        up = remote(piece, zu_s.at[part], z_r.at[z, part], (upper_z * 2 + core, tp))
+        down_copy = remote(piece, zd_s.at[part], z_r.at[z, part], (lower_z * 2 + core, tp))
+        pl.when(z < n_z - 1)(up.start)
+        pl.when(z > 0)(down_copy.start)
     whole = g.at[own_rows, :]
-    gc[0] = send(whole, whole, gc_s.at[0], gc_r.at[0], (other_core, tp))
+    gc = {0: send(whole, whole, gc_s, gc_r, (other_core, tp))}
+
+    distance = [jnp.maximum(z - q, q - z) for q in range(n_z)]
+    planes = [0] * n_z
+    for q in range(n_z):
+        rank = 0
+        for other in range(n_z):
+            nearer = (distance[other] <= distance[q]) if other < q else (distance[other] < distance[q])
+            rank = rank + jnp.where(nearer, 1, 0)
+        for slot in range(n_z):
+            planes[slot] = planes[slot] + jnp.where(rank == slot, q, 0)
+    middle = (z > 0) & (z < n_z - 1)
+    edge = jnp.logical_not(middle)
+
+    def z_forward(slot, part):
+        plane = planes[slot]
+        target = jnp.where(plane < z, z + 1, z - 1)
+        valid = (target >= 0) & (target < n_z)
+        safe = jnp.maximum(jnp.minimum(target, n_z - 1), 0)
+        piece = z_piece(plane, part, side)
+        return valid, remote(piece, zf_s.at[slot, part], z_r.at[plane, part], (safe * 2 + core, tp))
+
+    def e_copy(slot, part):
+        piece = z_piece(planes[slot], part, side)
+        return remote(piece, e_s.at[slot, part], e_r.at[slot, part], (ep, facing))
+
+    def d_copy(slot, part, late):
+        piece = z_piece(planes[slot], part, 1 - side if late else side)
+        return remote(piece, d_s.at[slot, late, part], d_r.at[slot, late, part], (other_core, tp))
+
+    def z_arrive(slot, part):
+        with jax.named_scope(f"z_arrive{slot}{part}"):
+            valid, forward = z_forward(slot, part)
+            forward.wait_recv()
+            pl.when(valid)(forward.start)
+            e_copy(slot, part).start()
+            d_copy(slot, part, 0).start()
+
+    def e_arrive(slot, part):
+        with jax.named_scope(f"e_arrive{slot}{part}"):
+            e_copy(slot, part).wait_recv()
+            d_copy(slot, part, 1).start()
+
+    def gather_drain():
+        for part in range(2):
+            piece = z_piece(z, part, side)
+            up = remote(piece, zu_s.at[part], z_r.at[z, part], (upper_z * 2 + core, tp))
+            down_copy = remote(piece, zd_s.at[part], z_r.at[z, part], (lower_z * 2 + core, tp))
+            pl.when(z < n_z - 1)(up.wait_send)
+            pl.when(z > 0)(down_copy.wait_send)
+            for slot in range(1, n_z):
+                valid, forward = z_forward(slot, part)
+                pl.when(valid)(forward.wait_send)
+                e_copy(slot, part).wait_send()
+                for late in range(2):
+                    d_copy(slot, part, late).wait_send()
 
     with jax.named_scope("shared"):
         loads[13].wait()
@@ -257,23 +330,24 @@
 
     channels = pin.shape[1]
     reach = halo_s.shape[0]
-    with jax.named_scope("pool_in"):
-        loads[0].wait()
-        loads[2].wait()
-        norm_into(mi, mg, mm, 0)
-        loads[4].wait()
-        pooled_in = jnp.dot(mm[...], pin[...], preferred_element_type=f32).astype(bf16)
-        halo_s[...] = pooled_in[rows - reach :]
-        ext[reach:, :] = pooled_in.astype(f32)
-        halo = send(halo_s, halo_r, h_s, h_r, ((ep + 1) % n_ep, tp))
+    def pool_project():
+        with jax.named_scope("pool_in"):
+            loads[0].wait()
+            loads[2].wait()
+            norm_into(mi, mg, mm, 0)
+            loads[4].wait()
+            pooled_in = jnp.dot(mm[...], pin[...], preferred_element_type=f32).astype(bf16)
+            halo_s[...] = pooled_in[rows - reach :]
+            ext[reach:, :] = pooled_in.astype(f32)
+            pl.when(ep < n_ep - 1)(halo.start)
 
     eye = lax.broadcasted_iota(jnp.int32, (rows, rows), 0) == lax.broadcasted_iota(
         jnp.int32, (rows, rows), 1
     )
 
     def window():
-        halo.wait_recv()
-        ext[:reach, :] = jnp.where(ep == 0, 0.0, halo_r[...].astype(f32))
+        pl.when(ep > 0)(halo.wait_recv)
+        ext[:reach, :] = halo_r[...].astype(f32)
         position = (ep * rows + 1 + lax.broadcasted_iota(jnp.int32, (rows, 1), 0)).astype(f32)
         total = jnp.zeros((rows, channels), f32)
         result = jnp.zeros((rows, channels), f32)
@@ -290,46 +364,28 @@
         sq_all[tp] = jnp.sum(jnp.where(eye, squares, 0.0), axis=0, keepdims=True)
         po_all[:, aligned(tp, channels)] = (scaled * pgain[...]).astype(bf16)
 
-    def block(k):
-        return ((z + n_z - k) % n_z) * 2 + core
-
-    def gathered(k, quarter):
-        return g.at[aligned(block(k), rows), aligned(quarter, cols)]
-
-    def gathered_half(k, part, quarter):
-        start = pl.multiple_of(block(k) * rows + part * half, half)
-        return g.at[pl.ds(start, half), aligned(quarter, cols)]
-
-    def across(k):
-        with jax.named_scope(f"across{k}"):
-            z_copies[k].wait_recv()
-            part = gathered(k, tp)
-            gx[k] = send(part, part, gx_s.at[k], gx_r.at[k], (ep, xn))
-            gy[k] = send(part, part, gy_s.at[k], gy_r.at[k], (ep, yn))
-
-    def corner(k):
-        with jax.named_scope(f"corner{k}"):
-            gx[k].wait_recv()
-            part = gathered_half(k, 0, xn)
-            gu[k] = send(part, part, gu_s.at[k], gu_r.at[k], (ep, yn))
-            gy[k].wait_recv()
-            part = gathered_half(k, 1, yn)
-            gv[k] = send(part, part, gv_s.at[k], gv_r.at[k], (ep, xn))
-
-    def over(k):
-        with jax.named_scope(f"over{k}"):
-            gu[k].wait_recv()
-            gv[k].wait_recv()
-            part = g.at[aligned(block(k), rows), :]
-            gc[k] = send(part, part, gc_s.at[k], gc_r.at[k], (other_core, tp))
-
     c_copies, dx_copies, dy_copies, x_copies, y_copies, f_copies = {}, {}, {}, {}, {}, {}
     fe = wg.shape[1]
 
     def compute(k):
-        plane = (z + n_z - k) % n_z
+        plane = planes[k]
         with jax.named_scope(f"wait_over{k}"):
-            gc[k].wait_recv()
+            if k == 0:
+                gc[0].wait_recv()
+            else:
+                for late in range(2):
+                    for part in range(2):
+                        d_copy(k, part, late).wait_recv()
+            for part in range(2):
+                source = plane * 2 + part
+
+                def arrive():
+                    remote(dense.at[source], w_s.at[1], w_r.at[source], (other_core, tp)).wait_recv()
+
+                if k == 0:
+                    pl.when(core != part)(arrive)
+                else:
+                    arrive()
         with jax.named_scope(f"hidden{k}"):
             pair = aligned(plane, 2 * rows)
             factors = []
@@ -394,11 +450,11 @@
                 s[k, :, aligned(tp, cols)].astype(f32) + qx[k].astype(f32) + qy[k].astype(f32)
             )
             if k == 0:
-                o[...] += total
+                o[...] = total
             else:
                 r[k] = total.astype(bf16)
                 f_copies[k] = send(
-                    r.at[k], bz.at[k], f_s.at[k], f_r.at[k], (((z + n_z - k) % n_z) * 2 + core, tp)
+                    r.at[k], bz.at[z], f_s.at[k], f_r.at[z], (planes[k] * 2 + core, tp)
                 )
 
     q_copies = []
@@ -412,7 +468,7 @@
                 copy.wait()
             loads[15].wait()
             loads[7].wait()
-            o[...] = jnp.dot(sh_all[...], sd[...], preferred_element_type=f32)
+            so[...] = jnp.dot(sh_all[...], sd[...], preferred_element_type=f32)
             mean = jnp.sum(sq_all[...], axis=0) / (channels * n_tp)
             inverse = lax.rsqrt(mean + epsilon)
             inverse = jnp.sum(jnp.where(eye, inverse, 0.0), axis=1, keepdims=True)
@@ -420,65 +476,83 @@
                 jnp.dot(po_all[...], pout[...], preferred_element_type=f32) * inverse
             ).astype(bf16)
 
-    with jax.named_scope("w_wait"):
-        for copy in w_copies:
-            copy.wait()
+    def pooling():
+        with jax.named_scope("window"):
+            window()
+        spread(1, po_all)
+        for number, t in enumerate(peers):
+            q_copies.append(send(sq_all.at[tp], sq_all.at[tp], q_s.at[number], q_r.at[number], (ep, t)))
+
+    def turn(condition, *steps):
+        def body():
+            for step, slot in steps:
+                for part in range(2):
+                    step(slot, part)
+
+        pl.when(condition)(body)
+
+    last = n_z - 1
     with jax.named_scope("weights_wait"):
         for number in (10, 11, 12):
             loads[number].wait()
-    with jax.named_scope("window"):
-        window()
-        spread(1, po_all)
-        for number, t in enumerate(peers):
-            q_copies.append(send(sq_all.at[tp], sq_all.at[tp], q_s.at[number], q_r.at[number], (ep, t)))
-
-    far = order[2:]
     compute(0)
-    across(order[0])
-    across(order[1])
+    z_arrive(1, 0)
+    pl.when(middle)(lambda: z_arrive(2, 0))
+    z_arrive(1, 1)
+    pl.when(middle)(lambda: z_arrive(2, 1))
+    pool_project()
+    first(0)
+    e_arrive(1, 0)
+    e_arrive(1, 1)
     with jax.named_scope("spread_corner"):
         spread_corner(0, sh_all)
+    pooling()
+    turn(middle, (e_arrive, 2))
+    pl.when(middle)(lambda: z_arrive(3, 0))
+    compute(1)
+    turn(edge, (z_arrive, 2))
+    pl.when(middle)(lambda: z_arrive(3, 1))
+    second(0)
+    first(1)
+    pl.when(edge)(lambda: z_arrive(3, 0))
+    turn(edge, (e_arrive, 2))
+    with jax.named_scope("spread_corner"):
         spread_corner(1, po_all)
-    first(0)
-    for k in far:
-        across(k)
-    corner(order[0])
-    corner(order[1])
-    over(order[0])
-    over(order[1])
-    second(0)
-    for k in far:
-        corner(k)
+    pl.when(edge)(lambda: z_arrive(3, 1))
+    turn(middle, (e_arrive, 3))
+    compute(2)
+    second(1)
+    turn(edge, (e_arrive, 3))
+    first(2)
+    third(0)
+    compute(3)
+    second(2)
+    third(1)
+    first(3)
     finish_t()
-    compute(order[0])
-    for k in far:
-        over(k)
-    first(order[0])
-    compute(order[1])
-    third(0)
-    second(order[0])
-    first(order[1])
-    todo = order[1:]
-    for k in far:
-        compute(k)
-        second(todo[0])
-        first(k)
-        third(order[order.index(todo[0]) - 1])
-        todo = todo[1:]
-    second(order[-1])
-    third(order[-2])
-    third(order[-1])
+    third(2)
+    second(3)
+    third(3)
     with jax.named_scope("final"):
-        for k in order[:-1]:
-            f_copies[k].wait_recv()
-            o[...] += bz[k].astype(f32)
-        f_copies[order[-1]].wait_recv()
-        moe_ref[...] = (o[...] + bz[order[-1]].astype(f32)).astype(bf16)
+        for k in range(1, n_z):
+            source = planes[k]
+            pltpu.make_async_remote_copy(
+                src_ref=r.at[k],
+                dst_ref=bz.at[source],
+                send_sem=f_s.at[k],
+                recv_sem=f_r.at[source],
+                device_id=(source * 2 + core, tp),
+                device_id_type=MESH,
+            ).wait_recv()
+            if k < last:
+                o[...] += bz[source].astype(f32)
+            else:
+                moe_ref[...] = (o[...] + so[...] + bz[source].astype(f32)).astype(bf16)
     with jax.named_scope("drain"):
-        halo.wait_send()
+        pl.when(ep < n_ep - 1)(halo.wait_send)
+        gather_drain()
         for group in (
-            z_copies, gx, gy, gu, gv, gc, t_copies,
-            c_copies, dx_copies, dy_copies, x_copies, y_copies, f_copies,
+            w_copies, gc, t_copies, c_copies, dx_copies, dy_copies, x_copies, y_copies, f_copies,
         ):
             for copy in group.values():
                 copy.wait_send()
@@ -549,12 +623,17 @@
         pltpu.VMEM((n_z, rows, cols), bf16),
         pltpu.VMEM((n_z, rows, cols), bf16),
         pltpu.VMEM((rows, cols), f32),
+        pltpu.VMEM((rows, cols), f32),
     ]
     dma = pltpu.SemaphoreType.DMA
     sems = (
         [dma((len(operands),))]
         + [dma((n_ep,))] * 2
-        + [dma((n_z,))] * 24
+        + [dma((2,))] * 2
+        + [dma((n_z, 2))] * 4
+        + [dma((n_z, 2, 2))] * 2
+        + [dma] * 2
+        + [dma((n_z,))] * 12
         + [dma((2, 4))] * 2
         + [dma((3,))] * 2
         + [dma] * 2
@@ -562,8 +641,8 @@
     return pl.pallas_call(
         lambda *refs: fused_kernel(n_ep, n_tp, *refs),
         out_shape=(
-            jax.ShapeDtypeStruct((rows, cols), bf16),
-            jax.ShapeDtypeStruct((rows, cols), bf16),
+            pltpu.VMEM((rows, cols), bf16),
+            pltpu.VMEM((rows, cols), bf16),
         ),
         in_specs=[pl.BlockSpec(memory_space=pltpu.HBM)] * len(operands),
         out_specs=(pl.BlockSpec(memory_space=pltpu.VMEM),) * 2,
@@ -573,13 +652,11 @@
         ),
         name="fused",
     )(*operands)
-
-
 def chosen(*arrays):
     route, expert_gate = arrays[8], arrays[10]
     experts = expert_gate.shape[0] * lax.axis_size("ep")
     capacity = 2 * route.shape[0] * route.shape[1] // experts
-    square = lax.axis_size("tp") == 4 and lax.axis_size("ep") >= 6
+    square = lax.axis_size("tp") == 4 and lax.axis_size("ep") == 2 * lax.axis_size("tp")
     if capacity == route.shape[0] and expert_gate.shape[0] == 1 and square:
         return dense_on_device(*arrays)
     return on_device(*arrays)

time: 72 us -> 58.5 us (0.81)
  Pallas kernels: 68 us -> 56.4 us
  local copies, waits for them, and re-layouts: 3.14 us -> 1.31 us
    pallas_call x1, Pallas kernels: 68 us -> 56.4 us  [dense_on_device(): pl.pallas_call(lambda *refs: fused_kernel(n_ep, n_tp, *refs), out_shape=(...]
    unnamed x2, local copies, waits for them, and re-layouts: 3.14 us -> 1.31 us
where the time goes in v2:
time: 58.5 us; the launch traced here: 58.3 us
  Pallas kernels  56.4 us (96%)
  local copies, waits for them, and re-layouts  1.31 us (2%)
  between operations  0.65 us (1%)
    pallas_call x1, Pallas kernels, dense_on_device(): pl.pallas_call(lambda *refs: fused_kernel(n_ep, n_tp, *refs), out_shape=(...  56.4 us
    unnamed x2, local copies, waits for them, and re-layouts  1.31 us

profile of v2, /device:TPU:0, one launch (start us, length us, event | category | flops | bytes accessed | tf_op | source)
XLA Modules:
  0.0 58.3 jit_solution(18268145438021865374)
XLA Ops:
  0.6 56.4 %fused.1 = (bf16[128,512]{1,0:T(8,128)(2,1)S(1)}, bf16[128,512]{1,0:T(8,128)(2,1)S(1)}) custom-call(bf16[128,2048]{1,0:T(8,128)(2,1)} %refs_0_.1, bf16[128,2048]{1,0:T(8,128)(2,1)} %refs_1_.1, f32[1,2048]{1,0:T(1,128)} %bitcast.12, f32[1,2048]{1,0:T(1,128)} %bitcast.13, bf16[2048,256]{1,0:T(8,128)(2,1)} %refs_4_.1, f32[1,256]{1,0:T(1,128)} %bitcast.16, ...), custom_call_target="tpu_custom_call" | custom-call | tf_op jit(solution)/shard_map/fused/pallas_call | solution.py:641
  57.0 0.7 %copy.20 = bf16[128,512]{1,0:T(8,128)(2,1)} copy(bf16[128,512]{1,0:T(8,128)(2,1)S(1)} %get-tuple-element.2) | data formatting | bytes 262144
  57.7 0.7 %copy.21 = bf16[128,512]{1,0:T(8,128)(2,1)} copy(bf16[128,512]{1,0:T(8,128)(2,1)S(1)} %get-tuple-element.3) | data formatting | bytes 262144

commit v3 on v2

--- a/solution.py
+++ b/solution.py
@@ -142,11 +142,18 @@
     (mi, ei, mg, eg, pin, pscale, pgain, pout, rt, sc, wg, wu, wd, sg, su, sd) = staged
     (g, dense, mm, halo_s, halo_r, ext, sh_all, po_all, sq_all, hid) = rest[:10]
     (p, ca, s, bx, by, qx, qy, r, bz, o, so) = rest[10:21]
-    l_sem = rest[21]
-    (w_s, w_r, zu_s, zd_s, zf_s, z_r, e_s, e_r, d_s, d_r, gc_s, gc_r) = rest[22:34]
-    (c_s, c_r, dx_s, dx_r, dy_s, dy_r, x_s, x_r, y_s, y_r, f_s, f_r, t_s, t_r, q_s, q_r, h_s, h_r) = rest[34:]
+    pool = rest[21]
     ep, tp, z, core, xn, yn, dg = places()
     n_z = n_ep // 2
+    last = n_z - 1
+    counts = semaphore_counts(n_ep, n_tp)
+    begins = {}
+    for name in counts:
+        begins[name] = sum(list(counts.values())[: list(counts).index(name)])
+
+    def sem(name, index=0):
+        return pool.at[begins[name] + index]
+
     rows, width = ei.shape
     cols = width // n_tp
     half = rows // 2
@@ -156,8 +163,8 @@
     low, high = pl.ds(0, half), pl.ds(half, half)
 
     loads = {}
-    for number in (8, 9, 1, 3, 0, 2, 4, 13, 14, 5, 6, 10, 11, 12, 15, 7):
-        loads[number] = pltpu.make_async_copy(hbm[number], staged[number], l_sem.at[number])
+    for number in (1, 3, 8, 9, 13, 14, 10, 11, 12, 0, 2, 4, 5, 6, 15, 7):
+        loads[number] = pltpu.make_async_copy(hbm[number], staged[number], sem("load", number))
         loads[number].start()
 
     def send(src, dst, sem_s, sem_r, device):
@@ -170,32 +177,81 @@
     halo = pltpu.make_async_remote_copy(
         src_ref=halo_s,
         dst_ref=halo_r,
-        send_sem=h_s,
-        recv_sem=h_r,
+        send_sem=sem("halo", 0),
+        recv_sem=sem("halo", 1),
         device_id=((ep + 1) % n_ep, tp),
         device_id_type=MESH,
     )
     halo_r[...] = jnp.zeros_like(halo_r)
     peers = (xn, yn, dg)
-    partners = [((ep + m) % n_ep, tp) for m in range(1, n_ep)] + [(ep, t) for t in peers]
+    upper_z, lower_z = jnp.minimum(z + 1, n_z - 1), jnp.maximum(z - 1, 0)
+    upper, lower = (upper_z * 2 + core, tp), (lower_z * 2 + core, tp)
+    has_upper, has_lower = z < n_z - 1, z > 0
     barrier = pltpu.get_barrier_semaphore()
-    for partner in partners:
+
+    def knock(partner):
         pl.semaphore_signal(barrier, inc=1, device_id=partner, device_id_type=MESH)
 
-    def norm_into(src, gain, dst, start):
+    for partner in ((other_core, tp), (ep, xn), (ep, yn)):
+        knock(partner)
+    pl.when(has_upper)(lambda: knock(upper))
+    pl.when(has_lower)(lambda: knock(lower))
+
+    def norm_into(src, gain, dst, start, first_row, n_rows):
         step = 16
 
         def some(index, carry):
-            values = src[aligned(index, step), :].astype(f32)
+            row = pl.multiple_of(first_row + index * step, step)
+            values = src[pl.ds(row, step), :].astype(f32)
             scale = lax.rsqrt(jnp.mean(values * values, axis=-1, keepdims=True) + epsilon)
-            dst[pl.ds(pl.multiple_of(start + index * step, step), step), :] = (
+            dst[pl.ds(pl.multiple_of(start + row, step), step), :] = (
                 values * scale * gain[...]
             ).astype(bf16)
             return carry
 
-        lax.fori_loop(0, rows // step, some, 0)
+        lax.fori_loop(0, n_rows // step, some, 0)
+
+    side = jnp.where(core == 0, tp % 2, tp // 2)
+    facing = jnp.where(core == 0, xn, yn)
+    wide = width // 2
+
+    def z_piece(plane, part, columns):
+        start = pl.multiple_of((plane * 2 + core) * rows + part * half, half)
+        return g.at[pl.ds(start, half), aligned(columns, wide)]
+
+    def remote(piece, sem_s, sem_r, device):
+        return pltpu.make_async_remote_copy(
+            src_ref=piece, dst_ref=piece, send_sem=sem_s, recv_sem=sem_r, device_id=device, device_id_type=MESH
+        )
+
+    def own_z(part):
+        piece = z_piece(z, part, side)
+        up = remote(piece, sem("own", 0), sem("z", z * 2 + part), upper)
+        low_copy = remote(piece, sem("own", 1), sem("z", z * 2 + part), lower)
+        return up, low_copy
+
+    def own_w():
+        up = remote(dense.at[ep], sem("w_own", 0), sem("w", ep), upper)
+        low_copy = remote(dense.at[ep], sem("w_own", 1), sem("w", ep), lower)
+        return up, low_copy
+
+    def start_own(pair):
+        pl.when(has_upper)(pair[0].start)
+        pl.when(has_lower)(pair[1].start)
 
     with jax.named_scope("norm"):
+        loads[1].wait()
+        loads[3].wait()
+        norm_into(ei, eg, g, ep * rows, 0, half)
+    with jax.named_scope("greet"):
+        pl.semaphore_wait(barrier, 3 + jnp.where(has_upper, 1, 0) + jnp.where(has_lower, 1, 0))
+    with jax.named_scope("norm2"):
+        start_own(own_z(0))
+        norm_into(ei, eg, g, ep * rows, half, half)
+        start_own(own_z(1))
+    whole = g.at[own_rows, :]
+    gc = {0: send(whole, whole, sem("sent"), sem("own_pair"), (other_core, tp))}
+    with jax.named_scope("dense"):
         loads[8].wait()
         loads[9].wait()
         total_score = jnp.sum(sc[...], axis=0, keepdims=True)
@@ -205,40 +261,11 @@
             share = 2.5 * sc[choice : choice + 1, :] / total_score
             mine = mine + jnp.where(rt[choice : choice + 1, :] == expert_ids, share, 0.0)
         dense[ep] = mine
-        loads[1].wait()
-        loads[3].wait()
-        norm_into(ei, eg, g, ep * rows)
-    with jax.named_scope("greet"):
-        pl.semaphore_wait(barrier, len(partners))
-    w_copies = {}
-    for m in range(1, n_ep):
-        target = ((z + m // 2) % n_z) * 2 + (core + m) % 2
-        w_copies[m] = send(dense.at[ep], dense.at[ep], w_s.at[m], w_r.at[ep], (target, tp))
-
-    side = jnp.where(core == 0, tp % 2, tp // 2)
-    facing = jnp.where(core == 0, xn, yn)
-    wide = width // 2
-
-    def z_piece(plane, part, columns):
-        start = pl.multiple_of((plane * 2 + core) * rows + part * half, half)
-        return g.at[pl.ds(start, half), aligned(columns, wide)]
-
-    def remote(piece, sem_s, sem_r, device):
-        return pltpu.make_async_remote_copy(
-            src_ref=piece, dst_ref=piece, send_sem=sem_s, recv_sem=sem_r, device_id=device, device_id_type=MESH
-        )
-
-    upper_z, lower_z = jnp.minimum(z + 1, n_z - 1), jnp.maximum(z - 1, 0)
-    for part in range(2):
-        piece = z_piece(z, part, side)
-        up = remote(piece, zu_s.at[part], z_r.at[z, part], (upper_z * 2 + core, tp))
-        down_copy = remote(piece, zd_s.at[part], z_r.at[z, part], (lower_z * 2 + core, tp))
-        pl.when(z < n_z - 1)(up.start)
-        pl.when(z > 0)(down_copy.start)
-    whole = g.at[own_rows, :]
-    gc = {0: send(whole, whole, gc_s, gc_r, (other_core, tp))}
-
-    distance = [jnp.maximum(z - q, q - z) for q in range(n_z)]
+        start_own(own_w())
+        send(dense.at[ep], dense.at[ep], sem("w_over"), sem("w", ep), (other_core, tp))
+
+    inner = jnp.where(2 * z < n_z, 1, -1)
+    distance = [2 * jnp.maximum(z - q, q - z) - jnp.where((q - z) * inner > 0, 1, 0) for q in range(n_z)]
     planes = [0] * n_z
     for q in range(n_z):
         rank = 0
@@ -249,6 +276,9 @@
             planes[slot] = planes[slot] + jnp.where(rank == slot, q, 0)
     middle = (z > 0) & (z < n_z - 1)
     edge = jnp.logical_not(middle)
+    near, far = planes[n_z - 2], planes[n_z - 1]
+    planes[n_z - 2] = jnp.where(middle, far, near)
+    planes[n_z - 1] = jnp.where(middle, near, far)
 
     def z_forward(slot, part):
         plane = planes[slot]
@@ -256,15 +286,24 @@
         valid = (target >= 0) & (target < n_z)
         safe = jnp.maximum(jnp.minimum(target, n_z - 1), 0)
         piece = z_piece(plane, part, side)
-        return valid, remote(piece, zf_s.at[slot, part], z_r.at[plane, part], (safe * 2 + core, tp))
+        return valid, remote(piece, sem("onward", slot - 1), sem("z", plane * 2 + part), (safe * 2 + core, tp))
+
+    def w_forward(slot):
+        plane = planes[slot]
+        target = jnp.where(plane < z, z + 1, z - 1)
+        safe = jnp.maximum(jnp.minimum(target, n_z - 1), 0)
+        source = plane * 2 + core
+        onward = remote(dense.at[source], sem("w_onward", slot - 1), sem("w", source), (safe * 2 + core, tp))
+        over = remote(dense.at[source], sem("w_over"), sem("w", source), (other_core, tp))
+        return onward, over
 
     def e_copy(slot, part):
         piece = z_piece(planes[slot], part, side)
-        return remote(piece, e_s.at[slot, part], e_r.at[slot, part], (ep, facing))
+        return remote(piece, sem("moved"), sem("e", (slot - 1) * 2 + part), (ep, facing))
 
     def d_copy(slot, part, late):
         piece = z_piece(planes[slot], part, 1 - side if late else side)
-        return remote(piece, d_s.at[slot, late, part], d_r.at[slot, late, part], (other_core, tp))
+        return remote(piece, sem("moved"), sem("d", slot - 1), (other_core, tp))
 
     def z_arrive(slot, part):
         with jax.named_scope(f"z_arrive{slot}{part}"):
@@ -273,25 +312,49 @@
             pl.when(valid)(forward.start)
             e_copy(slot, part).start()
             d_copy(slot, part, 0).start()
+            if part == 1:
+                onward, over = w_forward(slot)
+                onward.wait_recv()
+                pl.when(valid)(onward.start)
+                over.start()
 
     def e_arrive(slot, part):
         with jax.named_scope(f"e_arrive{slot}{part}"):
             e_copy(slot, part).wait_recv()
             d_copy(slot, part, 1).start()
 
+    def await_all(ref, name, index=0, received=False):
+        copy = pltpu.make_async_remote_copy(
+            src_ref=ref,
+            dst_ref=ref,
+            send_sem=sem(name, index),
+            recv_sem=sem(name, index),
+            device_id=(other_core, tp),
+            device_id_type=MESH,
+        )
+        if received:
+            copy.wait_recv()
+        else:
+            copy.wait_send()
+
+    def block_of(n_rows, n_columns):
+        return g.at[pl.ds(0, n_rows), pl.ds(0, n_columns)]
+
     def gather_drain():
-        for part in range(2):
-            piece = z_piece(z, part, side)
-            up = remote(piece, zu_s.at[part], z_r.at[z, part], (upper_z * 2 + core, tp))
-            down_copy = remote(piece, zd_s.at[part], z_r.at[z, part], (lower_z * 2 + core, tp))
-            pl.when(z < n_z - 1)(up.wait_send)
-            pl.when(z > 0)(down_copy.wait_send)
-            for slot in range(1, n_z):
-                valid, forward = z_forward(slot, part)
-                pl.when(valid)(forward.wait_send)
-                e_copy(slot, part).wait_send()
-                for late in range(2):
-                    d_copy(slot, part, late).wait_send()
+        def own_sent(number):
+            await_all(block_of(rows, wide), "own", number)
+            await_all(dense.at[0], "w_own", number)
+
+        def onward_sent(slot):
+            await_all(block_of(rows, wide), "onward", slot - 1)
+            await_all(dense.at[0], "w_onward", slot - 1)
+
+        pl.when(has_upper)(lambda: own_sent(0))
+        pl.when(has_lower)(lambda: own_sent(1))
+        for slot in range(1, n_z):
+            valid, _ = z_forward(slot, 0)
+            pl.when(valid)(lambda: onward_sent(slot))
+        await_all(dense.at[pl.ds(0, n_z)], "w_over")
 
     with jax.named_scope("shared"):
         loads[13].wait()
@@ -314,17 +377,21 @@
     def spread(kind, buffer):
         size = buffer.shape[1] // n_tp
         mine_slot = buffer.at[:, aligned(tp, size)]
-        t_copies[kind, 0] = send(mine_slot, mine_slot, t_s.at[kind, 0], t_r.at[kind, 0], (ep, xn))
-        t_copies[kind, 1] = send(mine_slot, mine_slot, t_s.at[kind, 1], t_r.at[kind, 1], (ep, yn))
+        t_copies[kind, 0] = send(mine_slot, mine_slot, sem("sent"), sem("t", kind * 3), (ep, xn))
+        t_copies[kind, 1] = send(mine_slot, mine_slot, sem("sent"), sem("t", kind * 3 + 1), (ep, yn))
 
     def spread_corner(kind, buffer):
         size = buffer.shape[1] // n_tp
         t_copies[kind, 0].wait_recv()
         part = buffer.at[low, aligned(xn, size)]
-        t_copies[kind, 2] = send(part, part, t_s.at[kind, 2], t_r.at[kind, 2], (ep, yn))
+        t_copies[kind, 2] = send(part, part, sem("sent"), sem("t", kind * 3 + 2), (ep, yn))
         t_copies[kind, 1].wait_recv()
         part = buffer.at[high, aligned(yn, size)]
-        t_copies[kind, 3] = send(part, part, t_s.at[kind, 3], t_r.at[kind, 3], (ep, xn))
+        t_copies[kind, 3] = send(part, part, sem("sent"), sem("t", kind * 3 + 2), (ep, xn))
+
+    def corner_arrived(kind, buffer):
+        size = buffer.shape[1] // n_tp
+        await_all(buffer.at[:, pl.ds(0, size)], "t", kind * 3 + 2, True)
 
     spread(0, sh_all)
 
@@ -334,7 +401,7 @@
         with jax.named_scope("pool_in"):
             loads[0].wait()
             loads[2].wait()
-            norm_into(mi, mg, mm, 0)
+            norm_into(mi, mg, mm, 0, 0, rows)
             loads[4].wait()
             pooled_in = jnp.dot(mm[...], pin[...], preferred_element_type=f32).astype(bf16)
             halo_s[...] = pooled_in[rows - reach :]
@@ -367,25 +434,15 @@
     c_copies, dx_copies, dy_copies, x_copies, y_copies, f_copies = {}, {}, {}, {}, {}, {}
     fe = wg.shape[1]
 
-    def compute(k):
+    def hidden(k):
         plane = planes[k]
         with jax.named_scope(f"wait_over{k}"):
             if k == 0:
                 gc[0].wait_recv()
             else:
-                for late in range(2):
-                    for part in range(2):
-                        d_copy(k, part, late).wait_recv()
-            for part in range(2):
-                source = plane * 2 + part
-
-                def arrive():
-                    remote(dense.at[source], w_s.at[1], w_r.at[source], (other_core, tp)).wait_recv()
-
-                if k == 0:
-                    pl.when(core != part)(arrive)
-                else:
-                    arrive()
+                await_all(block_of(rows, width), "d", k - 1, True)
+            source = plane * 2 + 1 - core
+            remote(dense.at[source], sem("w_own", 0), sem("w", source), (other_core, tp)).wait_recv()
         with jax.named_scope(f"hidden{k}"):
             pair = aligned(plane, 2 * rows)
             factors = []
@@ -393,79 +450,120 @@
                 line = dense[plane * 2 + part, pl.ds(ep, 1), :]
                 factors.append(jnp.sum(jnp.where(eye, line, 0.0), axis=1, keepdims=True))
             factor = jnp.concatenate(factors, axis=0)
-
-            def tile_hidden(index, carry):
-                part = aligned(index, tile)
+            for index in range(fe // tile):
+                part = pl.ds(index * tile, tile)
                 gate = jnp.dot(g[pair, :], wg[:, part], preferred_element_type=f32)
                 upper = jnp.dot(g[pair, :], wu[:, part], preferred_element_type=f32)
                 hid[:, part] = (gate / (1.0 + jnp.exp(-gate)) * upper * factor).astype(bf16)
-                return carry
-
-            lax.fori_loop(0, fe // tile, tile_hidden, 0)
+
+    quarters = (dg, yn, xn, tp)
+
+    def down(k):
         with jax.named_scope(f"down{k}"):
-
-            def tile_down(index, carry):
-                part = aligned(index, cols)
-                p[k, :, part] = jnp.dot(hid[...], wd[:, part], preferred_element_type=f32).astype(bf16)
-                return carry
-
-            lax.fori_loop(0, width // cols, tile_down, 0)
-            c_copies[k] = send(
-                p.at[k, aligned(1 - core, rows), :], ca.at[k], c_s.at[k], c_r.at[k], (other_core, tp)
-            )
+            if k < last:
+                for index in range(n_tp):
+                    part = pl.ds(index * cols, cols)
+                    p[k, :, part] = jnp.dot(hid[...], wd[:, part], preferred_element_type=f32).astype(bf16)
+            if k < last:
+                c_copies[k, 0] = send(
+                    p.at[k, aligned(1 - core, rows), :], ca.at[k], sem("sent"), sem("c", k), (other_core, tp)
+                )
+            else:
+                for number, quarter in enumerate(quarters):
+                    part = aligned(quarter, cols)
+                    p[k, :, part] = jnp.dot(hid[...], wd[:, part], preferred_element_type=f32).astype(bf16)
+                    c_copies[k, number] = send(
+                        p.at[k, aligned(1 - core, rows), part],
+                        ca.at[k, :, part],
+                        sem("sent"),
+                        sem("c", k + number),
+                        (other_core, tp),
+                    )
+
+    def cuts(k):
+        return 2 if k in (0, last) else 1
+
+    def place(k, cut):
+        return sum(cuts(other) for other in range(k)) + cut
+
+    def strip(k, quarter, cut):
+        size = cols // cuts(k)
+        return pl.ds(pl.multiple_of(quarter * cols + cut * size, size), size)
+
+    def local_strip(k, cut):
+        size = cols // cuts(k)
+        return pl.ds(cut * size, size)
+
+    def merge(k, number):
+        if (k, number) in c_copies:
+            c_copies[k, number].wait_recv()
+        part = aligned(quarters[number], cols)
+        s[k, :, part] = (
+            p[k, aligned(core, rows), part].astype(f32) + ca[k, :, part].astype(f32)
+        ).astype(bf16)
 
     def first(k):
         with jax.named_scope(f"first{k}"):
-            c_copies[k].wait_recv()
-            s[k] = (p[k, aligned(core, rows), :].astype(f32) + ca[k].astype(f32)).astype(bf16)
-            dx_copies[k] = send(
-                s.at[k, low, aligned(dg, cols)], bx.at[k], dx_s.at[k], dx_r.at[k], (ep, xn)
-            )
-            dy_copies[k] = send(
-                s.at[k, high, aligned(dg, cols)], by.at[k], dy_s.at[k], dy_r.at[k], (ep, yn)
-            )
+            merge(k, 0)
+            for cut in range(cuts(k)):
+                here, there = strip(k, dg, cut), local_strip(k, cut)
+                dx_copies[k, cut] = send(
+                    s.at[k, low, here], bx.at[k, :, there], sem("moved"), sem("dx", place(k, cut)), (ep, xn)
+                )
+                dy_copies[k, cut] = send(
+                    s.at[k, high, here], by.at[k, :, there], sem("moved"), sem("dy", place(k, cut)), (ep, yn)
+                )
+            for number in range(1, len(quarters)):
+                merge(k, number)
 
     def second(k):
         with jax.named_scope(f"second{k}"):
-            dx_copies[k].wait_recv()
-            s[k, low, aligned(yn, cols)] = (
-                s[k, low, aligned(yn, cols)].astype(f32) + bx[k].astype(f32)
-            ).astype(bf16)
-            y_copies[k] = send(
-                s.at[k, :, aligned(yn, cols)], qy.at[k], y_s.at[k], y_r.at[k], (ep, yn)
-            )
-            dy_copies[k].wait_recv()
-            s[k, high, aligned(xn, cols)] = (
-                s[k, high, aligned(xn, cols)].astype(f32) + by[k].astype(f32)
-            ).astype(bf16)
-            x_copies[k] = send(
-                s.at[k, :, aligned(xn, cols)], qx.at[k], x_s.at[k], x_r.at[k], (ep, xn)
-            )
+            for cut in range(cuts(k)):
+                there = local_strip(k, cut)
+                here = strip(k, yn, cut)
+                dx_copies[k, cut].wait_recv()
+                s[k, low, here] = (
+                    s[k, low, here].astype(f32) + bx[k, :, there].astype(f32)
+                ).astype(bf16)
+                y_copies[k, cut] = send(
+                    s.at[k, :, here], qy.at[k, :, there], sem("moved"), sem("xy", place(k, cut)), (ep, yn)
+                )
+                here = strip(k, xn, cut)
+                dy_copies[k, cut].wait_recv()
+                s[k, high, here] = (
+                    s[k, high, here].astype(f32) + by[k, :, there].astype(f32)
+                ).astype(bf16)
+                x_copies[k, cut] = send(
+                    s.at[k, :, here], qx.at[k, :, there], sem("moved"), sem("xy", place(k, cut)), (ep, xn)
+                )
 
     def third(k):
         with jax.named_scope(f"third{k}"):
-            x_copies[k].wait_recv()
-            y_copies[k].wait_recv()
-            total = (
-                s[k, :, aligned(tp, cols)].astype(f32) + qx[k].astype(f32) + qy[k].astype(f32)
-            )
-            if k == 0:
-                o[...] = total
-            else:
-                r[k] = total.astype(bf16)
-                f_copies[k] = send(
-                    r.at[k], bz.at[z], f_s.at[k], f_r.at[z], (planes[k] * 2 + core, tp)
+            for cut in range(cuts(k)):
+                there = local_strip(k, cut)
+                await_all(block_of(2 * rows, cols // cuts(k)), "xy", place(k, cut), True)
+                total = (
+                    s[k, :, strip(k, tp, cut)].astype(f32)
+                    + qx[k, :, there].astype(f32)
+                    + qy[k, :, there].astype(f32)
                 )
-
-    q_copies = []
+                if k == 0:
+                    o[:, there] = total
+                else:
+                    r[k, :, there] = total.astype(bf16)
+                    f_copies[k, cut] = send(
+                        r.at[k, :, there],
+                        bz.at[z, :, there],
+                        sem("sent"),
+                        sem("f", z),
+                        (planes[k] * 2 + core, tp),
+                    )
+
 
     def finish_t():
         with jax.named_scope("epilogue"):
-            for kind in range(2):
-                t_copies[kind, 2].wait_recv()
-                t_copies[kind, 3].wait_recv()
-            for copy in q_copies:
-                copy.wait()
+            corner_arrived(1, po_all)
+            await_all(sq_all.at[pl.ds(0, n_tp - 1)], "squares", 1, True)
             loads[15].wait()
             loads[7].wait()
             so[...] = jnp.dot(sh_all[...], sd[...], preferred_element_type=f32)
@@ -476,86 +574,102 @@
                 jnp.dot(po_all[...], pout[...], preferred_element_type=f32) * inverse
             ).astype(bf16)
 
+    def spread_squares(number):
+        line = sq_all.at[tp]
+        send(line, line, sem("squares", 0), sem("squares", 1), (ep, peers[number]))
+
     def pooling():
         with jax.named_scope("window"):
             window()
         spread(1, po_all)
-        for number, t in enumerate(peers):
-            q_copies.append(send(sq_all.at[tp], sq_all.at[tp], q_s.at[number], q_r.at[number], (ep, t)))
-
-    def turn(condition, *steps):
-        def body():
-            for step, slot in steps:
-                for part in range(2):
-                    step(slot, part)
-
-        pl.when(condition)(body)
-
-    last = n_z - 1
+        for number in range(2):
+            spread_squares(number)
+
     with jax.named_scope("weights_wait"):
         for number in (10, 11, 12):
             loads[number].wait()
-    compute(0)
+    def on_edge(step, *which):
+        pl.when(edge)(lambda: step(*which))
+
+    def on_middle(step, *which):
+        pl.when(middle)(lambda: step(*which))
+
+    hidden(0)
+    down(0)
     z_arrive(1, 0)
-    pl.when(middle)(lambda: z_arrive(2, 0))
+    on_middle(z_arrive, 3, 0)
+    pool_project()
     z_arrive(1, 1)
-    pl.when(middle)(lambda: z_arrive(2, 1))
-    pool_project()
-    first(0)
+    on_middle(z_arrive, 3, 1)
+    with jax.named_scope("spread_corner"):
+        spread_corner(0, sh_all)
     e_arrive(1, 0)
     e_arrive(1, 1)
-    with jax.named_scope("spread_corner"):
-        spread_corner(0, sh_all)
     pooling()
-    turn(middle, (e_arrive, 2))
-    pl.when(middle)(lambda: z_arrive(3, 0))
-    compute(1)
-    turn(edge, (z_arrive, 2))
-    pl.when(middle)(lambda: z_arrive(3, 1))
-    second(0)
+    z_arrive(2, 0)
+    hidden(1)
+    down(1)
+    z_arrive(2, 1)
     first(1)
-    pl.when(edge)(lambda: z_arrive(3, 0))
-    turn(edge, (e_arrive, 2))
     with jax.named_scope("spread_corner"):
         spread_corner(1, po_all)
-    pl.when(edge)(lambda: z_arrive(3, 1))
-    turn(middle, (e_arrive, 3))
-    compute(2)
+        corner_arrived(0, sh_all)
+        spread_squares(2)
+    e_arrive(2, 0)
+    on_edge(z_arrive, 3, 0)
     second(1)
-    turn(edge, (e_arrive, 3))
+    e_arrive(2, 1)
+    hidden(2)
+    on_edge(z_arrive, 3, 1)
+    down(2)
+    e_arrive(3, 0)
     first(2)
-    third(0)
-    compute(3)
+    third(1)
+    e_arrive(3, 1)
+    hidden(3)
     second(2)
-    third(1)
+    down(3)
     first(3)
-    finish_t()
+    first(0)
     third(2)
     second(3)
+    second(0)
+    finish_t()
     third(3)
+    third(0)
     with jax.named_scope("final"):
+        o[...] += so[...]
         for k in range(1, n_z):
             source = planes[k]
             pltpu.make_async_remote_copy(
                 src_ref=r.at[k],
                 dst_ref=bz.at[source],
-                send_sem=f_s.at[k],
-                recv_sem=f_r.at[source],
+                send_sem=sem("sent"),
+                recv_sem=sem("f", source),
                 device_id=(source * 2 + core, tp),
                 device_id_type=MESH,
             ).wait_recv()
             if k < last:
                 o[...] += bz[source].astype(f32)
             else:
-                moe_ref[...] = (o[...] + so[...] + bz[source].astype(f32)).astype(bf16)
+                moe_ref[...] = (o[...] + bz[source].astype(f32)).astype(bf16)
     with jax.named_scope("drain"):
         pl.when(ep < n_ep - 1)(halo.wait_send)
         gather_drain()
-        for group in (
-            w_copies, gc, t_copies, c_copies, dx_copies, dy_copies, x_copies, y_copies, f_copies,
-        ):
-            for copy in group.values():
-                copy.wait_send()
+        await_all(sq_all.at[pl.ds(0, n_tp - 1)], "squares", 0)
+        shared_rows = 3 * half * (sh_all.shape[1] + po_all.shape[1]) // (n_tp * width) * 2
+        await_all(block_of((n_z + 1) * rows + last * rows // n_tp + shared_rows, width), "sent")
+        await_all(block_of(3 * half * last + 3 * half * n_z * 2 // n_tp, width), "moved")
+
+
+def semaphore_counts(n_ep, n_tp):
+    n_z = n_ep // 2
+    return {
+        "load": 16, "own": 2, "w_own": 2, "onward": n_z - 1, "w_onward": n_z - 1, "w_over": 1,
+        "sent": 1, "moved": 1, "z": 2 * n_z, "w": n_ep, "own_pair": 1, "e": 2 * (n_z - 1),
+        "d": n_z - 1, "c": n_z - 1 + n_tp, "dx": n_z + 2, "dy": n_z + 2, "xy": n_z + 2, "f": n_z,
+        "t": 6, "squares": 2, "halo": 2,
+    }
 
 
 def dense_on_device(
@@ -625,19 +739,7 @@
         pltpu.VMEM((rows, cols), f32),
         pltpu.VMEM((rows, cols), f32),
     ]
-    dma = pltpu.SemaphoreType.DMA
-    sems = (
-        [dma((len(operands),))]
-        + [dma((n_ep,))] * 2
-        + [dma((2,))] * 2
-        + [dma((n_z, 2))] * 4
-        + [dma((n_z, 2, 2))] * 2
-        + [dma] * 2
-        + [dma((n_z,))] * 12
-        + [dma((2, 4))] * 2
-        + [dma((3,))] * 2
-        + [dma] * 2
-    )
+    sems = [pltpu.SemaphoreType.DMA((sum(semaphore_counts(n_ep, n_tp).values()),))]
     return pl.pallas_call(
         lambda *refs: fused_kernel(n_ep, n_tp, *refs),
         out_shape=(

time: 58.5 us -> 54.3 us (0.928)
  Pallas kernels: 56.4 us -> 52.2 us
    pallas_call x1, Pallas kernels: 56.4 us -> 52.2 us  [dense_on_device(): pl.pallas_call(lambda *refs: fused_kernel(n_ep, n_tp, *refs), out_shape=(...]
where the time goes in v3:
time: 54.3 us; the launch traced here: 54.2 us
  Pallas kernels  52.2 us (96%)
  local copies, waits for them, and re-layouts  1.31 us (2%)
  between operations  0.65 us (1%)
    pallas_call x1, Pallas kernels, dense_on_device(): pl.pallas_call(lambda *refs: fused_kernel(n_ep, n_tp, *refs), out_shape=(...  52.2 us
    unnamed x2, local copies, waits for them, and re-layouts  1.31 us

profile of v3, /device:TPU:0, one launch (start us, length us, event | category | flops | bytes accessed | tf_op | source)
XLA Modules:
  0.0 54.2 jit_solution(8889446668491683626)
XLA Ops:
  0.6 52.2 %fused.1 = (bf16[128,512]{1,0:T(8,128)(2,1)S(1)}, bf16[128,512]{1,0:T(8,128)(2,1)S(1)}) custom-call(bf16[128,2048]{1,0:T(8,128)(2,1)} %refs_0_.1, bf16[128,2048]{1,0:T(8,128)(2,1)} %refs_1_.1, f32[1,2048]{1,0:T(1,128)} %bitcast.12, f32[1,2048]{1,0:T(1,128)} %bitcast.13, bf16[2048,256]{1,0:T(8,128)(2,1)} %refs_4_.1, f32[1,256]{1,0:T(1,128)} %bitcast.16, ...), custom_call_target="tpu_custom_call" | custom-call | tf_op jit(solution)/shard_map/fused/pallas_call | solution.py:743
  52.8 0.7 %copy.20 = bf16[128,512]{1,0:T(8,128)(2,1)} copy(bf16[128,512]{1,0:T(8,128)(2,1)S(1)} %get-tuple-element.2) | data formatting | bytes 262144
  53.5 0.7 %copy.21 = bf16[128,512]{1,0:T(8,128)(2,1)} copy(bf16[128,512]{1,0:T(8,128)(2,1)S(1)} %get-tuple-element.3) | data formatting | bytes 262144

commit v4 on v3

--- a/solution.py
+++ b/solution.py
@@ -136,13 +136,13 @@
 
 
 def fused_kernel(n_ep, n_tp, *refs):
-    hbm, (mix_ref, moe_ref), rest = refs[:16], refs[16:18], refs[18:]
+    hbm, out_ref, rest = refs[:16], refs[16], refs[17:]
     (mi_h, ei_h, mg_h, eg_h, pi_h, ps_h, pg_h, po_h, rt_h, sc_h, wg_h, wu_h, wd_h, sg_h, su_h, sd_h) = hbm
     staged, rest = rest[:16], rest[16:]
     (mi, ei, mg, eg, pin, pscale, pgain, pout, rt, sc, wg, wu, wd, sg, su, sd) = staged
     (g, dense, mm, halo_s, halo_r, ext, sh_all, po_all, sq_all, hid) = rest[:10]
-    (p, ca, s, bx, by, qx, qy, r, bz, o, so) = rest[10:21]
-    pool = rest[21]
+    (p, ca, s, bx, by, qx, qy, r, bz, o, so, lifted) = rest[10:22]
+    pool = rest[22]
     ep, tp, z, core, xn, yn, dg = places()
     n_z = n_ep // 2
     last = n_z - 1
@@ -183,6 +183,7 @@
         device_id_type=MESH,
     )
     halo_r[...] = jnp.zeros_like(halo_r)
+    lifted[...] = jnp.zeros_like(lifted)
     peers = (xn, yn, dg)
     upper_z, lower_z = jnp.minimum(z + 1, n_z - 1), jnp.maximum(z - 1, 0)
     upper, lower = (upper_z * 2 + core, tp), (lower_z * 2 + core, tp)
@@ -224,11 +225,35 @@
             src_ref=piece, dst_ref=piece, send_sem=sem_s, recv_sem=sem_r, device_id=device, device_id_type=MESH
         )
 
+    middle = has_upper & has_lower
+    edge = jnp.logical_not(middle)
+
     def own_z(part):
         piece = z_piece(z, part, side)
         up = remote(piece, sem("own", 0), sem("z", z * 2 + part), upper)
         low_copy = remote(piece, sem("own", 1), sem("z", z * 2 + part), lower)
         return up, low_copy
+
+    def start_own_z(part):
+        up, low_copy = own_z(part)
+        pl.when(middle)(up.start)
+        pl.when(middle)(low_copy.start)
+        inner = jnp.where(has_upper, upper_z, lower_z)
+        straight = remote(
+            z_piece(z, part, side), sem("own", 0), sem("z", z * 2 + part), (inner * 2 + core, tp)
+        )
+        pl.when(edge)(straight.start)
+
+    def start_rest():
+        inner = jnp.where(has_upper, upper_z, lower_z)
+        for part in range(2):
+            rest_copy = remote(
+                z_piece(z, part, 1 - side),
+                sem("own", 0),
+                sem("e", (last - 1) * 2 + part),
+                (inner * 2 + core, tp),
+            )
+            pl.when(edge)(rest_copy.start)
 
     def own_w():
         up = remote(dense.at[ep], sem("w_own", 0), sem("w", ep), upper)
@@ -246,9 +271,9 @@
     with jax.named_scope("greet"):
         pl.semaphore_wait(barrier, 3 + jnp.where(has_upper, 1, 0) + jnp.where(has_lower, 1, 0))
     with jax.named_scope("norm2"):
-        start_own(own_z(0))
+        start_own_z(0)
         norm_into(ei, eg, g, ep * rows, half, half)
-        start_own(own_z(1))
+        start_own_z(1)
     whole = g.at[own_rows, :]
     gc = {0: send(whole, whole, sem("sent"), sem("own_pair"), (other_core, tp))}
     with jax.named_scope("dense"):
@@ -274,8 +299,6 @@
             rank = rank + jnp.where(nearer, 1, 0)
         for slot in range(n_z):
             planes[slot] = planes[slot] + jnp.where(rank == slot, q, 0)
-    middle = (z > 0) & (z < n_z - 1)
-    edge = jnp.logical_not(middle)
     near, far = planes[n_z - 2], planes[n_z - 1]
     planes[n_z - 2] = jnp.where(middle, far, near)
     planes[n_z - 1] = jnp.where(middle, near, far)
@@ -305,18 +328,22 @@
         piece = z_piece(planes[slot], part, 1 - side if late else side)
         return remote(piece, sem("moved"), sem("d", slot - 1), (other_core, tp))
 
-    def z_arrive(slot, part):
+    def z_arrive(slot, part, exchange=True):
         with jax.named_scope(f"z_arrive{slot}{part}"):
             valid, forward = z_forward(slot, part)
             forward.wait_recv()
             pl.when(valid)(forward.start)
-            e_copy(slot, part).start()
+            if exchange:
+                e_copy(slot, part).start()
             d_copy(slot, part, 0).start()
             if part == 1:
                 onward, over = w_forward(slot)
                 onward.wait_recv()
                 pl.when(valid)(onward.start)
                 over.start()
+
+    def full_arrive(slot, part):
+        z_arrive(slot, part, False)
 
     def e_arrive(slot, part):
         with jax.named_scope(f"e_arrive{slot}{part}"):
@@ -342,13 +369,15 @@
 
     def gather_drain():
         def own_sent(number):
-            await_all(block_of(rows, wide), "own", number)
             await_all(dense.at[0], "w_own", number)
 
         def onward_sent(slot):
             await_all(block_of(rows, wide), "onward", slot - 1)
             await_all(dense.at[0], "w_onward", slot - 1)
 
+        pl.when(middle)(lambda: await_all(block_of(rows, wide), "own", 0))
+        pl.when(middle)(lambda: await_all(block_of(rows, wide), "own", 1))
+        pl.when(edge)(lambda: await_all(block_of(rows, width), "own", 0))
         pl.when(has_upper)(lambda: own_sent(0))
         pl.when(has_lower)(lambda: own_sent(1))
         for slot in range(1, n_z):
@@ -377,21 +406,22 @@
     def spread(kind, buffer):
         size = buffer.shape[1] // n_tp
         mine_slot = buffer.at[:, aligned(tp, size)]
-        t_copies[kind, 0] = send(mine_slot, mine_slot, sem("sent"), sem("t", kind * 3), (ep, xn))
-        t_copies[kind, 1] = send(mine_slot, mine_slot, sem("sent"), sem("t", kind * 3 + 1), (ep, yn))
+        t_copies[kind, 0] = send(mine_slot, mine_slot, sem("sent"), sem("t", kind * 4), (ep, xn))
+        t_copies[kind, 1] = send(mine_slot, mine_slot, sem("sent"), sem("t", kind * 4 + 1), (ep, yn))
 
     def spread_corner(kind, buffer):
         size = buffer.shape[1] // n_tp
         t_copies[kind, 0].wait_recv()
         part = buffer.at[low, aligned(xn, size)]
-        t_copies[kind, 2] = send(part, part, sem("sent"), sem("t", kind * 3 + 2), (ep, yn))
+        t_copies[kind, 2] = send(part, part, sem("sent"), sem("t", kind * 4 + 2), (ep, yn))
         t_copies[kind, 1].wait_recv()
         part = buffer.at[high, aligned(yn, size)]
-        t_copies[kind, 3] = send(part, part, sem("sent"), sem("t", kind * 3 + 2), (ep, xn))
+        t_copies[kind, 3] = send(part, part, sem("sent"), sem("t", kind * 4 + 3), (ep, xn))
 
     def corner_arrived(kind, buffer):
         size = buffer.shape[1] // n_tp
-        await_all(buffer.at[:, pl.ds(0, size)], "t", kind * 3 + 2, True)
+        for number in (2, 3):
+            await_all(buffer.at[low, pl.ds(0, size)], "t", kind * 4 + number, True)
 
     spread(0, sh_all)
 
@@ -431,7 +461,7 @@
         sq_all[tp] = jnp.sum(jnp.where(eye, squares, 0.0), axis=0, keepdims=True)
         po_all[:, aligned(tp, channels)] = (scaled * pgain[...]).astype(bf16)
 
-    c_copies, dx_copies, dy_copies, x_copies, y_copies, f_copies = {}, {}, {}, {}, {}, {}
+    c_copies = {}
     fe = wg.shape[1]
 
     def hidden(k):
@@ -498,42 +528,64 @@
         if (k, number) in c_copies:
             c_copies[k, number].wait_recv()
         part = aligned(quarters[number], cols)
-        s[k, :, part] = (
-            p[k, aligned(core, rows), part].astype(f32) + ca[k, :, part].astype(f32)
-        ).astype(bf16)
+        own, theirs = p[k, aligned(core, rows), part].astype(f32), ca[k, :, part].astype(f32)
+        if k == 0:
+            own = own + lifted[:, part].astype(f32)
+        s[k, :, part] = (own + theirs).astype(bf16)
 
     def first(k):
         with jax.named_scope(f"first{k}"):
             merge(k, 0)
             for cut in range(cuts(k)):
                 here, there = strip(k, dg, cut), local_strip(k, cut)
-                dx_copies[k, cut] = send(
+                send(
                     s.at[k, low, here], bx.at[k, :, there], sem("moved"), sem("dx", place(k, cut)), (ep, xn)
                 )
-                dy_copies[k, cut] = send(
+                send(
                     s.at[k, high, here], by.at[k, :, there], sem("moved"), sem("dy", place(k, cut)), (ep, yn)
                 )
             for number in range(1, len(quarters)):
                 merge(k, number)
+
+    def lift():
+        inner = jnp.where(has_upper, upper_z, lower_z)
+        return pltpu.make_async_remote_copy(
+            src_ref=s.at[1],
+            dst_ref=lifted,
+            send_sem=sem("lift", 0),
+            recv_sem=sem("lift", 1),
+            device_id=(inner * 2 + core, tp),
+            device_id_type=MESH,
+        )
+
+    def lift_start():
+        with jax.named_scope("lift"):
+            for number in range(len(quarters)):
+                merge(1, number)
+            lift().start()
+
+    def lift_arrive():
+        with jax.named_scope("lift_wait"):
+            lift().wait_recv()
 
     def second(k):
         with jax.named_scope(f"second{k}"):
             for cut in range(cuts(k)):
                 there = local_strip(k, cut)
                 here = strip(k, yn, cut)
-                dx_copies[k, cut].wait_recv()
+                await_all(bx.at[k, :, there], "dx", place(k, cut), True)
                 s[k, low, here] = (
                     s[k, low, here].astype(f32) + bx[k, :, there].astype(f32)
                 ).astype(bf16)
-                y_copies[k, cut] = send(
+                send(
                     s.at[k, :, here], qy.at[k, :, there], sem("moved"), sem("xy", place(k, cut)), (ep, yn)
                 )
                 here = strip(k, xn, cut)
-                dy_copies[k, cut].wait_recv()
+                await_all(by.at[k, :, there], "dy", place(k, cut), True)
                 s[k, high, here] = (
                     s[k, high, here].astype(f32) + by[k, :, there].astype(f32)
                 ).astype(bf16)
-                x_copies[k, cut] = send(
+                send(
                     s.at[k, :, here], qx.at[k, :, there], sem("moved"), sem("xy", place(k, cut)), (ep, xn)
                 )
 
@@ -551,7 +603,7 @@
                     o[:, there] = total
                 else:
                     r[k, :, there] = total.astype(bf16)
-                    f_copies[k, cut] = send(
+                    send(
                         r.at[k, :, there],
                         bz.at[z, :, there],
                         sem("sent"),
@@ -570,7 +622,7 @@
             mean = jnp.sum(sq_all[...], axis=0) / (channels * n_tp)
             inverse = lax.rsqrt(mean + epsilon)
             inverse = jnp.sum(jnp.where(eye, inverse, 0.0), axis=1, keepdims=True)
-            mix_ref[...] = (
+            out_ref[:rows] = (
                 jnp.dot(po_all[...], pout[...], preferred_element_type=f32) * inverse
             ).astype(bf16)
 
@@ -597,10 +649,11 @@
     hidden(0)
     down(0)
     z_arrive(1, 0)
-    on_middle(z_arrive, 3, 0)
+    start_rest()
+    on_middle(full_arrive, 3, 0)
     pool_project()
     z_arrive(1, 1)
-    on_middle(z_arrive, 3, 1)
+    on_middle(full_arrive, 3, 1)
     with jax.named_scope("spread_corner"):
         spread_corner(0, sh_all)
     e_arrive(1, 0)
@@ -608,28 +661,31 @@
     pooling()
     z_arrive(2, 0)
     hidden(1)
+    z_arrive(2, 1)
     down(1)
-    z_arrive(2, 1)
-    first(1)
+    on_edge(lift_start)
+    on_middle(first, 1)
     with jax.named_scope("spread_corner"):
         spread_corner(1, po_all)
-        corner_arrived(0, sh_all)
+        for number in (2, 3):
+            t_copies[0, number].wait_recv()
         spread_squares(2)
     e_arrive(2, 0)
     on_edge(z_arrive, 3, 0)
-    second(1)
+    on_edge(z_arrive, 3, 1)
+    on_middle(second, 1)
     e_arrive(2, 1)
     hidden(2)
-    on_edge(z_arrive, 3, 1)
     down(2)
     e_arrive(3, 0)
     first(2)
-    third(1)
     e_arrive(3, 1)
     hidden(3)
     second(2)
+    on_middle(third, 1)
     down(3)
     first(3)
+    on_middle(lift_arrive)
     first(0)
     third(2)
     second(3)
@@ -639,7 +695,8 @@
     third(0)
     with jax.named_scope("final"):
         o[...] += so[...]
-        for k in range(1, n_z):
+
+        def collect(k):
             source = planes[k]
             pltpu.make_async_remote_copy(
                 src_ref=r.at[k],
@@ -649,17 +706,31 @@
                 device_id=(source * 2 + core, tp),
                 device_id_type=MESH,
             ).wait_recv()
-            if k < last:
-                o[...] += bz[source].astype(f32)
-            else:
-                moe_ref[...] = (o[...] + bz[source].astype(f32)).astype(bf16)
+            o[...] += bz[source].astype(f32)
+
+        for k in range(1, last):
+            collect(k)
+        pl.when(edge)(lambda: collect(last))
+        out_ref[rows:] = o[...].astype(bf16)
     with jax.named_scope("drain"):
         pl.when(ep < n_ep - 1)(halo.wait_send)
         gather_drain()
         await_all(sq_all.at[pl.ds(0, n_tp - 1)], "squares", 0)
         shared_rows = 3 * half * (sh_all.shape[1] + po_all.shape[1]) // (n_tp * width) * 2
-        await_all(block_of((n_z + 1) * rows + last * rows // n_tp + shared_rows, width), "sent")
-        await_all(block_of(3 * half * last + 3 * half * n_z * 2 // n_tp, width), "moved")
+        sent_rows = (n_z + 1) * rows + last * rows // n_tp + shared_rows
+        moved_rows = 3 * half * last + 3 * half * n_z * 2 // n_tp
+
+        def middle_sent():
+            await_all(block_of(sent_rows, width), "sent")
+            await_all(block_of(moved_rows - half, width), "moved")
+
+        def edge_sent():
+            await_all(block_of(sent_rows - rows // n_tp, width), "sent")
+            await_all(block_of(moved_rows - 3 * half * 2 // n_tp, width), "moved")
+            await_all(lifted, "lift", 0)
+
+        pl.when(middle)(middle_sent)
+        pl.when(edge)(edge_sent)
 
 
 def semaphore_counts(n_ep, n_tp):
@@ -668,7 +739,7 @@
         "load": 16, "own": 2, "w_own": 2, "onward": n_z - 1, "w_onward": n_z - 1, "w_over": 1,
         "sent": 1, "moved": 1, "z": 2 * n_z, "w": n_ep, "own_pair": 1, "e": 2 * (n_z - 1),
         "d": n_z - 1, "c": n_z - 1 + n_tp, "dx": n_z + 2, "dy": n_z + 2, "xy": n_z + 2, "f": n_z,
-        "t": 6, "squares": 2, "halo": 2,
+        "t": 8, "squares": 2, "halo": 2, "lift": 2,
     }
 
 
@@ -738,22 +809,21 @@
         pltpu.VMEM((n_z, rows, cols), bf16),
         pltpu.VMEM((rows, cols), f32),
         pltpu.VMEM((rows, cols), f32),
+        pltpu.VMEM((rows, width), bf16),
     ]
     sems = [pltpu.SemaphoreType.DMA((sum(semaphore_counts(n_ep, n_tp).values()),))]
-    return pl.pallas_call(
+    both = pl.pallas_call(
         lambda *refs: fused_kernel(n_ep, n_tp, *refs),
-        out_shape=(
-            pltpu.VMEM((rows, cols), bf16),
-            pltpu.VMEM((rows, cols), bf16),
-        ),
+        out_shape=pltpu.VMEM((2 * rows, cols), bf16),
         in_specs=[pl.BlockSpec(memory_space=pltpu.HBM)] * len(operands),
-        out_specs=(pl.BlockSpec(memory_space=pltpu.VMEM),) * 2,
+        out_specs=pl.BlockSpec(memory_space=pltpu.VMEM),
         scratch_shapes=scratch + sems,
         compiler_params=pltpu.CompilerParams(
             collective_id=0, has_side_effects=True, vmem_limit_bytes=60 << 20
         ),
         name="fused",
     )(*operands)
+    return both[:rows], both[rows:]
 def chosen(*arrays):
     route, expert_gate = arrays[8], arrays[10]
     experts = expert_gate.shape[0] * lax.axis_size("ep")

time: 54.3 us -> 52.1 us (0.959)
  Pallas kernels: 52.2 us -> 50.6 us
  local copies, waits for them, and re-layouts: 1.31 us -> 0.72 us
    pallas_call x1, Pallas kernels: 52.2 us -> 50.6 us  [dense_on_device(): pl.pallas_call(lambda *refs: fused_kernel(n_ep, n_tp, *refs), out_shape=p...]
    unnamed x2 -> x0, local copies, waits for them, and re-layouts: 1.31 us -> none
    slice x0 -> x1, local copies, waits for them, and re-layouts: none -> 0.72 us  [dense_on_device(): return (both[:rows], both[rows:])]
where the time goes in v4:
time: 52.1 us; the launch traced here: 52 us
  Pallas kernels  50.6 us (97%)
  local copies, waits for them, and re-layouts  0.72 us (1%)
  between operations  0.64 us (1%)
    pallas_call x1, Pallas kernels, dense_on_device(): pl.pallas_call(lambda *refs: fused_kernel(n_ep, n_tp, *refs), out_shape=p...  50.6 us

profile of v4, /device:TPU:0, one launch (start us, length us, event | category | flops | bytes accessed | tf_op | source)
XLA Modules:
  0.0 52.0 jit_solution(17129709376545419803)
XLA Ops:
  0.6 50.6 %fused.1 = bf16[256,512]{1,0:T(8,128)(2,1)S(1)} custom-call(bf16[128,2048]{1,0:T(8,128)(2,1)} %refs_0_.1, bf16[128,2048]{1,0:T(8,128)(2,1)} %refs_1_.1, f32[1,2048]{1,0:T(1,128)} %bitcast.12, f32[1,2048]{1,0:T(1,128)} %bitcast.13, bf16[2048,256]{1,0:T(8,128)(2,1)} %refs_4_.1, f32[1,256]{1,0:T(1,128)} %bitcast.16, f32[1,256]{1,0:T(1,128)} %bitcast.17, ...), custom_call_target="tpu_custom_call" | custom-call | tf_op jit(solution)/shard_map/fused/pallas_call | solution.py:815
  51.3 0.7 %fusion = (bf16[128,512]{1,0:T(8,128)(2,1)}, bf16[128,512]{1,0:T(8,128)(2,1)}) fusion(bf16[256,512]{1,0:T(8,128)(2,1)S(1)} %fused.1), kind=kLoop, calls=%fused_computation | loop fusion | bytes 524288 | tf_op jit(solution)/shard_map/slice | solution.py:826

commit v5 on v4

--- a/solution.py
+++ b/solution.py
@@ -511,7 +511,7 @@
                     )
 
     def cuts(k):
-        return 2 if k in (0, last) else 1
+        return 1 if k == 1 else 2
 
     def place(k, cut):
         return sum(cuts(other) for other in range(k)) + cut
@@ -673,13 +673,14 @@
     e_arrive(2, 0)
     on_edge(z_arrive, 3, 0)
     on_edge(z_arrive, 3, 1)
-    on_middle(second, 1)
     e_arrive(2, 1)
     hidden(2)
+    on_middle(second, 1)
     down(2)
+    finish_t()
     e_arrive(3, 0)
+    e_arrive(3, 1)
     first(2)
-    e_arrive(3, 1)
     hidden(3)
     second(2)
     on_middle(third, 1)
@@ -690,7 +691,6 @@
     third(2)
     second(3)
     second(0)
-    finish_t()
     third(3)
     third(0)
     with jax.named_scope("final"):
@@ -738,7 +738,7 @@
     return {
         "load": 16, "own": 2, "w_own": 2, "onward": n_z - 1, "w_onward": n_z - 1, "w_over": 1,
         "sent": 1, "moved": 1, "z": 2 * n_z, "w": n_ep, "own_pair": 1, "e": 2 * (n_z - 1),
-        "d": n_z - 1, "c": n_z - 1 + n_tp, "dx": n_z + 2, "dy": n_z + 2, "xy": n_z + 2, "f": n_z,
+        "d": n_z - 1, "c": n_z - 1 + n_tp, "dx": 2 * n_z - 1, "dy": 2 * n_z - 1, "xy": 2 * n_z - 1, "f": n_z,
         "t": 8, "squares": 2, "halo": 2, "lift": 2,
     }
 

time: 52.1 us -> 51.1 us (0.981)
  Pallas kernels: 50.6 us -> 49.6 us
    pallas_call x1, Pallas kernels: 50.6 us -> 49.6 us  [dense_on_device(): pl.pallas_call(lambda *refs: fused_kernel(n_ep, n_tp, *refs), out_shape=p...]
where the time goes in v5:
time: 51.1 us; the launch traced here: 50.9 us
  Pallas kernels  49.6 us (97%)
  local copies, waits for them, and re-layouts  0.72 us (1%)
  between operations  0.64 us (1%)
    pallas_call x1, Pallas kernels, dense_on_device(): pl.pallas_call(lambda *refs: fused_kernel(n_ep, n_tp, *refs), out_shape=p...  49.6 us

profile of v5, /device:TPU:0, one launch (start us, length us, event | category | flops | bytes accessed | tf_op | source)
XLA Modules:
  0.0 50.9 jit_solution(13066784972582368892)
XLA Ops:
  0.6 49.6 %fused.1 = bf16[256,512]{1,0:T(8,128)(2,1)S(1)} custom-call(bf16[128,2048]{1,0:T(8,128)(2,1)} %refs_0_.1, bf16[128,2048]{1,0:T(8,128)(2,1)} %refs_1_.1, f32[1,2048]{1,0:T(1,128)} %bitcast.12, f32[1,2048]{1,0:T(1,128)} %bitcast.13, bf16[2048,256]{1,0:T(8,128)(2,1)} %refs_4_.1, f32[1,256]{1,0:T(1,128)} %bitcast.16, f32[1,256]{1,0:T(1,128)} %bitcast.17, ...), custom_call_target="tpu_custom_call" | custom-call | tf_op jit(solution)/shard_map/fused/pallas_call | solution.py:815
  50.2 0.7 %fusion = (bf16[128,512]{1,0:T(8,128)(2,1)}, bf16[128,512]{1,0:T(8,128)(2,1)}) fusion(bf16[256,512]{1,0:T(8,128)(2,1)S(1)} %fused.1), kind=kLoop, calls=%fused_computation | loop fusion | bytes 524288 | tf_op jit(solution)/shard_map/slice | solution.py:826
